TPU v7x, 32 devices: a whole 2x2x4 slice. The times are simulated.
32 devices in a mesh: rep: 2 (over x), fs: 8 (over z, y), tp: 2 (over core).
Axes of the slice: x: 2, y: 2, z: 4, core: 2. Of those that a mesh axis runs over, the one named last changes fastest.
Arguments:
- tokens: bfloat16 [12288, 2048], P(('rep', 'fs', 'tp')), may hold values from -6 to 6
- norm_gain: float32 [2048], replicated, may hold values from 0.1 to 1.9
- gate_weight: float32 [2048, 5632], P('fs', 'tp'), may hold values from -0.125 to 0.125
- up_weight: float32 [2048, 5632], P('fs', 'tp'), may hold values from -0.125 to 0.125
- gate_scale: float32 [5632], P('tp'), may hold values from 0.3 to 3
- up_scale: float32 [5632], P('tp'), may hold values from 0.3 to 3
- down_weight: float32 [5632, 2048], P('tp', 'fs'), may hold values from -0.078125 to 0.078125
- down_scale: float32 [2048], replicated, may hold values from 0.3 to 3
Outputs:
- mixed: bfloat16 [12288, 2048], P(('rep', 'fs', 'tp'))
All inputs are finite; a program needn't handle non-finite values.
Results may differ from a plain program's by a relative error of at most 0.014.
Values may be sent and summed in bfloat16 or wider, within the bound.
No kernel may reach another device: no remote copies, remote signals or barrier semaphores. Data moves between devices by JAX's collectives and lax.ppermute only.
A program may use at most 128 MiB of HBM per device.

v0:
```python
import jax
import jax.numpy as jnp
from jax import lax
from jax.sharding import PartitionSpec as P


def on_device(
    tokens, norm_gain, gate_weight, up_weight, gate_scale, up_scale, down_weight, down_scale
):
    values = tokens.astype(jnp.float32)
    own_normed = (
        values * lax.rsqrt(jnp.mean(values * values, axis=-1, keepdims=True) + 1e-06) * norm_gain
    ).astype(jnp.bfloat16)
    normed = lax.all_gather(own_normed, "tp", axis=0, tiled=True)
    gate_local = gate_weight.astype(jnp.bfloat16)
    up_local = up_weight.astype(jnp.bfloat16)
    gate_whole, up_whole = (
        lax.all_gather(gate_local, "fs", axis=0, tiled=True),
        lax.all_gather(up_local, "fs", axis=0, tiled=True),
    )
    gate_value = jnp.dot(normed, gate_whole, preferred_element_type=jnp.float32)
    up_value = jnp.dot(normed, up_whole, preferred_element_type=jnp.float32)
    hidden = (jax.nn.silu(gate_value * gate_scale) * (up_value * up_scale)).astype(jnp.bfloat16)
    partial_value = jnp.dot(
        hidden,
        lax.all_gather(down_weight.astype(jnp.bfloat16), "fs", axis=1, tiled=True),
        preferred_element_type=jnp.float32,
    )
    partial_value = partial_value.astype(jnp.bfloat16).astype(jnp.float32)
    summed = lax.psum_scatter(
        partial_value.astype(jnp.bfloat16), "tp", scatter_dimension=0, tiled=True
    ).astype(jnp.float32)
    return (summed * down_scale).astype(jnp.bfloat16)


def solution(mesh):
    placed = (
        P(("rep", "fs", "tp"), None),
        P(),
        P("fs", "tp"),
        P("fs", "tp"),
        P("tp"),
        P("tp"),
        P("tp", "fs"),
        P(),
    )
    return jax.shard_map(
        on_device,
        mesh=mesh,
        in_specs=placed,
        out_specs=P(("rep", "fs", "tp"), None),
        check_vma=False,
    )
```

profile of v0, /device:TPU:0, one launch (start us, length us, event | category | flops | bytes accessed | tf_op | source)
XLA Modules:
  0.0 569.5 jit_solution(4407416434645859061)
XLA Ops:
  6.5 0.0 copy-start
  6.5 0.0 all-gather.5.cloned.1.call-start
  6.5 1.9 fusion.4
  8.5 3.0 fusion.6
  11.5 0.0 all-gather.5.cloned.1.call-update
  11.5 0.0 all-gather.7.cloned.1.call-start
  11.5 0.0 copy-done
  11.6 1.3 convert_element_type.31
  12.8 0.0 all-gather.7.cloned.1.call-update
  12.9 0.0 copy-start.1
  12.9 0.0 all-gather.11.cloned.1.call-start
  12.9 3.2 convert_element_type.34
  16.2 0.0 all-gather.11.cloned.1.call-update
  16.2 0.0 all-gather.9.cloned.1.call-start
  16.2 0.0 copy-done.1
  16.2 1.3 convert_element_type.32
  17.5 0.0 all-gather.9.cloned.1.call-update
  17.5 0.0 copy-start.4
  17.5 0.0 copy-start.5
  17.5 0.0 reduce-scatter.2.cloned.1.call-start
  17.6 8.9 %all-gather.5.cloned.1.call-done = bf16[768,2048]{1,0:T(8,128)(2,1)} async-done(((bf16[384,2048]{1,0:T(8,128)(2,1)}), bf16[768,2048]{1,0:T(8,128)(2,1)}) %all-gather.5.cloned.1.call-update) | async-done | bytes 3145744 | tf_op jit(solution)/shard_map/all_gather | solution.py:14
  26.5 0.0 copy-start.3
  26.5 166.7 %all-gather.7.cloned.1.call-done = bf16[2048,2816]{1,0:T(8,128)(2,1)} async-done(((bf16[256,2816]{1,0:T(8,128)(2,1)}), bf16[2048,2816]{1,0:T(8,128)(2,1)}) %all-gather.7.cloned.1.call-update) | async-done | bytes 11534352 | tf_op jit(solution)/shard_map/all_gather | solution.py:18
  193.2 15.7 %fusion.8 = f32[768,2816]{1,0:T(8,128)} fusion(bf16[768,2048]{1,0:T(8,128)(2,1)} %all-gather.5.cloned.1.call-done, bf16[2048,2816]{1,0:T(8,128)(2,1)} %all-gather.7.cloned.1.call-done), kind=kOutput, calls=%fused_computation.13 | convolution fusion | flops 8858370048 | bytes 23330816 | tf_op jit(solution)/shard_map/dot_general | solution.py:21
  208.9 147.9 %all-gather.11.cloned.1.call-done = bf16[2816,2048]{1,0:T(8,128)(2,1)} async-done(((bf16[2816,256]{1,0:T(8,128)(2,1)}), bf16[2816,2048]{1,0:T(8,128)(2,1)}) %all-gather.11.cloned.1.call-update) | async-done | bytes 11534352 | tf_op jit(solution)/shard_map/all_gather | solution.py:26
  356.8 163.6 %all-gather.9.cloned.1.call-done = bf16[2048,2816]{1,0:T(8,128)(2,1)} async-done(((bf16[256,2816]{1,0:T(8,128)(2,1)}), bf16[2048,2816]{1,0:T(8,128)(2,1)}) %all-gather.9.cloned.1.call-update) | async-done | bytes 11534352 | tf_op jit(solution)/shard_map/all_gather | solution.py:19
  520.4 0.0 copy-done.4
  520.4 0.0 copy-done.5
  520.4 0.0 copy-done.3
  520.4 30.1 %fusion.3 = bf16[768,2048]{1,0:T(8,128)(2,1)} fusion(bf16[2816,2048]{1,0:T(8,128)(2,1)} %all-gather.11.cloned.1.call-done, f32[768,2816]{1,0:T(8,128)} %fusion.8, bf16[768,2048]{1,0:T(8,128)(2,1)S(1)} %copy-done.3, bf16[2048,2816]{1,0:T(8,128)(2,1)} %all-gather.9.cloned.1.call-done, f32[2816]{0:T(1024)S(1)} %copy-done.4, f32[2816]{0:T(1024)S(1)} %copy-done.5), kind=kOutput, calls=%fused_computation.6 | convolution fusion | flops 17735614464 | bytes 38033408 | tf_op jit(solution)/shard_map/dot_general | solution.py:24
  550.5 0.0 copy-start.2
  550.5 0.0 reduce-scatter.2.cloned.1.call-update
  550.5 9.5 %reduce-scatter.2.cloned.1.call-done = bf16[384,2048]{1,0:T(8,128)(2,1)} async-done(((bf16[768,2048]{1,0:T(8,128)(2,1)}), bf16[384,2048]{1,0:T(8,128)(2,1)}) %reduce-scatter.2.cloned.1.call-update) | async-done | bytes 1572880 | tf_op jit(solution)/shard_map/reduce_scatter | solution.py:30
  560.0 0.0 copy-done.2
  560.0 2.9 multiply_convert_fusion.1
  (1 shorter events, 0.0 us)
Async XLA Ops:
  6.5 5.0 copy-start
  6.5 20.0 %all-gather.5.cloned.1.call-start = ((), (), s32[]{:S(2)}) async-start(), calls=%async_computation.1 | async-start | bytes 4718592 | tf_op jit(solution)/shard_map/all_gather | solution.py:14
  11.5 181.7 %all-gather.7.cloned.1.call-start = ((), (), s32[]{:S(2)}) async-start(), calls=%async_computation.2 | async-start | bytes 12976128 | tf_op jit(solution)/shard_map/all_gather | solution.py:18
  12.9 3.4 copy-start.1
  12.9 344.0 %all-gather.11.cloned.1.call-start = ((), (), s32[]{:S(2)}) async-start(), calls=%async_computation.4 | async-start | bytes 12976128 | tf_op jit(solution)/shard_map/all_gather | solution.py:26
  16.2 504.2 %all-gather.9.cloned.1.call-start = ((), (), s32[]{:S(2)}) async-start(), calls=%async_computation.3 | async-start | bytes 12976128 | tf_op jit(solution)/shard_map/all_gather | solution.py:19
  17.5 502.9 %copy-start.4 = (f32[2816]{0:T(1024)S(1)}, f32[2816]{0:T(1024)}, u32[]{:S(2)}) copy-start(f32[2816]{0:T(1024)} %param.13) | copy-start | bytes 33796
  17.5 502.9 %copy-start.5 = (f32[2816]{0:T(1024)S(1)}, f32[2816]{0:T(1024)}, u32[]{:S(2)}) copy-start(f32[2816]{0:T(1024)} %param.12) | copy-start | bytes 33796
  17.5 542.5 %reduce-scatter.2.cloned.1.call-start = ((), (), s32[]{:S(2)}) async-start(), calls=%async_computation.5 | async-start | bytes 4718592 | tf_op jit(solution)/shard_map/reduce_scatter | solution.py:30
  26.5 493.9 %copy-start.3 = (bf16[768,2048]{1,0:T(8,128)(2,1)S(1)}, bf16[768,2048]{1,0:T(8,128)(2,1)}, u32[]{:S(2)}) copy-start(bf16[768,2048]{1,0:T(8,128)(2,1)} %all-gather.5.cloned.1.call-done) | copy-start | bytes 9437188
  550.5 9.5 %copy-start.2 = (f32[2048]{0:T(1024)S(1)}, f32[2048]{0:T(1024)}, u32[]{:S(2)}) copy-start(f32[2048]{0:T(1024)} %param.15) | copy-start | bytes 24580
Sparse Core Ops, SparseCore 0:
  11.6 14.8 all-gather.4
  28.7 164.4 all-gather.6
  195.3 161.5 all-gather.10
  358.9 161.4 all-gather.8
  550.6 9.3 reduce-scatter.1
where the time goes:
time: 570 us
  waiting for transfers between devices  497 us (87%)
  matrix products  45.8 us (8%)
  other arithmetic  13.6 us (2%)
  between operations  13.2 us (2%)
    all_gather x1, waiting for transfers between devices, on_device(): lax.all_gather(gate_local, 'fs', axis=0, tiled=True)  167 us
    all_gather x1, waiting for transfers between devices, on_device(): lax.all_gather(up_local, 'fs', axis=0, tiled=True)  164 us
    all_gather x1, waiting for transfers between devices, on_device(): lax.all_gather(down_weight.astype(jnp.bfloat16), 'fs', axis=1, tiled=True)  148 us
    dot_general x1, matrix products, on_device(): jnp.dot(hidden, lax.all_gather(down_weight.astype(jnp.bfloat16), 'fs', ax...  30.1 us
    dot_general x1, matrix products, on_device(): gate_value = jnp.dot(normed, gate_whole, preferred_element_type=jnp.float32)  15.7 us
  transfers between devices with their start and end apart: 5, of which 5 were waited for; matrix products, arithmetic and copies ran while one was open for 4% of the time, Pallas kernels for 0%

commit v1 on v0

v1 whole, which is shorter than its diff:
```python
import functools

import jax
import jax.numpy as jnp
from jax import lax
from jax.experimental import pallas as pl
from jax.experimental.pallas import tpu as pltpu
from jax.sharding import Mesh
from jax.sharding import PartitionSpec as P


BF16 = jnp.bfloat16
F32 = jnp.float32
LANES = 128
EPS = 1e-06


def general_plan(
    tokens, norm_gain, gate_weight, up_weight, gate_scale, up_scale, down_weight, down_scale
):
    values = tokens.astype(F32)
    own_normed = (
        values * lax.rsqrt(jnp.mean(values * values, axis=-1, keepdims=True) + EPS) * norm_gain
    ).astype(BF16)
    normed = lax.all_gather(own_normed, "tp", axis=0, tiled=True)
    gate_whole = lax.all_gather(gate_weight.astype(BF16), "fs", axis=0, tiled=True)
    up_whole = lax.all_gather(up_weight.astype(BF16), "fs", axis=0, tiled=True)
    gate_value = jnp.dot(normed, gate_whole, preferred_element_type=F32)
    up_value = jnp.dot(normed, up_whole, preferred_element_type=F32)
    hidden = (jax.nn.silu(gate_value * gate_scale) * (up_value * up_scale)).astype(BF16)
    down_whole = lax.all_gather(down_weight.astype(BF16), "fs", axis=1, tiled=True)
    partial_value = jnp.dot(hidden, down_whole, preferred_element_type=F32).astype(BF16)
    summed = lax.psum_scatter(partial_value, "tp", scatter_dimension=0, tiled=True).astype(F32)
    return (summed * down_scale).astype(BF16)


def pick(index, table):
    value = jnp.int32(table[0])
    for at, entry in enumerate(table[1:], 1):
        value = jnp.where(index == at, jnp.int32(entry), value)
    return value


def ring_order(count):
    return list(range(0, count, 2)) + list(range(1, count, 2))[::-1]


def ring_source(count, step):
    ring = ring_order(count)
    return [ring[(ring.index(z) - step) % count] for z in range(count)]


VM = pl.BlockSpec(memory_space=pltpu.VMEM)
ANY = pl.BlockSpec(memory_space=pl.ANY)


def call(kernel, outs, ins, *, flops=0, nbytes=0, **kw):
    kw.setdefault("in_specs", [VM] * len(ins))
    kw.setdefault("out_specs", [VM] * len(outs))
    return pl.pallas_call(
        kernel,
        out_shape=[jax.ShapeDtypeStruct(s, d) for s, d in outs],
        cost_estimate=pl.CostEstimate(
            flops=int(flops), bytes_accessed=int(nbytes), transcendentals=0
        ),
        **kw,
    )(*ins)


def norm_kernel(lo, t_ref, g_ref, lo_ref, hi_ref):
    rows = t_ref.shape[0]
    for at in range(0, rows, lo):
        v = t_ref[at : at + lo, :].astype(F32)
        v = v * lax.rsqrt(jnp.mean(v * v, axis=-1, keepdims=True) + EPS) * g_ref[...]
        if at == 0:
            lo_ref[...] = v.astype(BF16)
        else:
            hi_ref[at - lo : at, :] = v.astype(BF16)


def mixed(gr, ur, q, full):
    at = pl.multiple_of(4 * full + (q // 2) * LANES, LANES)
    odd = (q % 2) == 1
    g, u = gr[:, pl.ds(at, LANES)], ur[:, pl.ds(at, LANES)]
    half = LANES // 2
    g = jnp.where(odd, pltpu.roll(g, half, 1), g)
    u = jnp.where(odd, u, pltpu.roll(u, half, 1))
    lane = lax.broadcasted_iota(jnp.int32, g.shape, 1)
    return jnp.where(lane < half, g, u)


def take(gr, ur, q, full, first, one, two):
    second = full - first
    at = pl.multiple_of(q * full, LANES)
    later = pl.multiple_of(q * full + first, LANES)
    kind = one.dtype
    one[:, :first] = gr[:, pl.ds(at, first)].astype(kind)
    one[:, first:] = ur[:, pl.ds(at, first)].astype(kind)
    two[:, :second] = gr[:, pl.ds(later, second)].astype(kind)
    two[:, second : 2 * second] = ur[:, pl.ds(later, second)].astype(kind)
    two[:, 2 * second :] = mixed(gr, ur, q, full).astype(kind)


def prep_kernel(full, first, g_ref, u_ref, own1, own2, far1, far2):
    x, y = lax.axis_index("x"), lax.axis_index("y")
    take(g_ref, u_ref, 2 * x + y, full, first, own1, own2)
    take(g_ref, u_ref, 2 * x + 1 - y, full, first, far1, far2)


def scale_kernel(full, first, g_ref, u_ref, out):
    x, y = lax.axis_index("x"), lax.axis_index("y")
    take(g_ref, u_ref, 2 * x + y, full, first, out.at[:, : 2 * first], out.at[:, 2 * first :])


def down_prep_kernel(full, d_ref, own, other):
    x, y = lax.axis_index("x"), lax.axis_index("y")
    half = LANES // 2
    for q, out in ((2 * x + y, own), (2 * x + 1 - y, other)):
        out[:full, :] = d_ref[pl.ds(pl.multiple_of(q * full, 64), full), :].astype(BF16)
        out[full:, :] = d_ref[pl.ds(pl.multiple_of(4 * full + q * half, 64), half), :].astype(BF16)


def gate_up_kernel(nz, blk, part, x_ref, s_own, s_oth, *refs):
    pieces, (out, w, wsem) = refs[: 4 * nz], refs[4 * nz :]
    y, z = lax.axis_index("y"), lax.axis_index("z")
    n = s_own.shape[1]

    @pl.when(pl.program_id(0) == 0)
    def _():
        copies = []
        for s in range(nz):
            f = 2 * pick(z, ring_source(nz, s)) + y
            b = 2 * pick(z, ring_source(nz, -s)) + 1 - y
            for k, at in enumerate((f, b, f, b)):
                rows = pl.ds(pl.multiple_of(at * blk, blk), blk)
                dst = w.at[rows, pl.ds(n * (k // 2), n)]
                copies.append(pltpu.make_async_copy(pieces[k * nz + s], dst, wsem.at[4 * s + k]))
        for c in copies:
            c.start()
        for c in copies:
            c.wait()

    value = jnp.dot(x_ref[...], w[...], preferred_element_type=F32)
    tails = []
    for at, scale in ((0, s_own), (1, s_oth)):
        v = value[:, at * n : (at + 1) * n] * scale[...]
        g, u = v[:, :part], v[:, part : 2 * part]
        out[:, at * part : (at + 1) * part] = (g / (1 + jnp.exp(-g)) * u).astype(BF16)
        if n > 2 * part:
            m = v[:, 2 * part :]
            tails.append(m / (1 + jnp.exp(-m)) * pltpu.roll(m, LANES // 2, 1))
    if tails:
        h, o = tails
        lane = lax.broadcasted_iota(jnp.int32, h.shape, 1)
        o = pltpu.roll(o, LANES // 2, 1)
        out[:, 2 * part :] = jnp.where(lane < LANES // 2, h, o).astype(BF16)


def down_kernel(cuts, h1, h2, a_own, a_oth, b_own, b_oth, ax_keep, ax_send, ay_keep, ay_send, w):
    i = pl.program_id(0)
    blk = a_own.shape[1]

    @pl.when(i == 0)
    def _():
        at = 0
        for lo, hi in cuts:
            for own, left in ((True, at), (False, at + hi - lo)):
                w[left : left + hi - lo, :blk] = (a_own if own else a_oth)[lo:hi, :]
                w[left : left + hi - lo, blk:] = (b_own if own else b_oth)[lo:hi, :]
            at += 2 * (hi - lo)

    n = h1.shape[1]
    value = jnp.dot(h1[...], w[:n], preferred_element_type=F32) + jnp.dot(
        h2[...], w[n:], preferred_element_type=F32
    )
    value = value.astype(BF16)
    left, right = value[:, :blk], value[:, blk:]

    @pl.when(i < 2)
    def _():
        ax_keep[0] = left

    @pl.when(i >= 2)
    def _():
        ax_send[0] = left

    @pl.when(i % 2 == 0)
    def _():
        ay_keep[0] = right

    @pl.when(i % 2 == 1)
    def _():
        ay_send[0] = right


def second_add_kernel(ax_keep, ax_got, ay_keep, ay_got, ax, ay):
    ax[...] = (ax_keep[0].astype(F32) + ax_got[0].astype(F32)).astype(BF16)
    ay[...] = (ay_keep[0].astype(F32) + ay_got[0].astype(F32)).astype(BF16)


def final_kernel(nz, blk, *refs):
    ins, scale, out = refs[:-2], refs[-2], refs[-1]
    z = lax.axis_index("z")
    for s in range(nz):
        for j in range(2):
            a, b, c = ins[6 * s + 3 * j : 6 * s + 3 * j + 3]
            source = pick(z, ring_source(nz, s if j == 0 else -s))
            at = pl.ds(pl.multiple_of((2 * source + j) * blk, blk), blk)
            value = a[0].astype(F32) + b[0].astype(F32) + c[...].astype(F32)
            out[:, at] = (value * scale[:, at]).astype(BF16)


def after(value, *others):
    return lax.optimization_barrier((value, *others))[0]


def pair_plan(
    nz, tokens, norm_gain, gate_weight, up_weight, gate_scale, up_scale, down_weight, down_scale
):
    rows, width = tokens.shape
    blk, ffl = gate_weight.shape
    full = ffl // (4 * LANES) * LANES
    quarter = ffl // 4
    first = max(LANES, full - LANES)
    second = full - first
    wide1, wide2 = 2 * first, 2 * second + LANES
    lo = rows // 3
    ring = ring_order(nz)
    ahead = [(ring[p], ring[(p + 1) % nz]) for p in range(nz)]
    back = [(b, a) for a, b in ahead]
    swap = [(0, 1), (1, 0)]
    y = lax.axis_index("y")

    def send(v, axis, hops=swap):
        return lax.ppermute(v, axis, hops)

    own1, own2, far1, far2 = call(
        functools.partial(prep_kernel, full, first),
        [((blk, wide1), BF16), ((blk, wide2), BF16)] * 2,
        [gate_weight, up_weight],
        flops=blk * ffl * 2,
        nbytes=blk * ffl * 12,
    )
    hop = lambda v: send(v, "z", ahead)
    pop = lambda v: send(v, "z", back)
    c1, c2 = [own1, hop(own1)], [own2, hop(own2)]
    g1 = [send(far1, "y")]
    n_lo, n_hi = call(
        functools.partial(norm_kernel, lo),
        [((lo, width), BF16), ((rows - lo, width), BF16)],
        [after(tokens, own1), norm_gain.reshape(1, -1)],
        flops=rows * width * 8,
        nbytes=rows * width * 4,
    )
    hi_x, hi_y = send(n_hi, "x"), send(n_hi, "y")
    d_own, d_nbr = call(
        functools.partial(down_prep_kernel, full),
        [((quarter, blk), BF16), ((quarter, blk), BF16)],
        [after(down_weight, n_hi)],
        flops=blk * ffl,
        nbytes=blk * ffl * 6,
    )
    (scale,) = call(
        functools.partial(scale_kernel, full, first),
        [((1, 2 * quarter), F32)],
        [after(gate_scale, d_own).reshape(1, -1), after(up_scale, d_own).reshape(1, -1)],
        flops=ffl,
        nbytes=ffl * 8,
    )
    scale_oth = send(scale, "c")
    clock = d_own

    def event(value):
        nonlocal clock
        clock = after(value, clock)
        return clock

    across = {}

    def twin(name, v):
        across[name] = send(v, "c")

    twin("c10", own1)
    twin("c20", own2)
    c1[1] = event(c1[1])
    c1.append(hop(c1[1]))
    twin("c11", c1[1])
    lo_x = send(after(n_lo, clock), "x")
    g1[0] = event(g1[0])
    g1.append(pop(g1[0]))
    twin("g10", g1[0])
    g2 = [send(after(far2, clock), "y")]
    c2[1] = event(c2[1])
    twin("c21", c2[1])
    lo_y = send(after(n_lo, clock), "y")
    c1[2] = event(c1[2])
    c1.append(hop(c1[2]))
    twin("c12", c1[2])
    hi_x = event(hi_x)
    g1[1] = event(g1[1])
    g1.append(pop(g1[1]))
    twin("g11", g1[1])
    hi_y = event(hi_y)
    hi_xy = send(hi_y, "x")
    lo_x = event(lo_x)
    lo_xy = send(lo_x, "y")
    g2[0] = event(g2[0])
    twin("g20", g2[0])
    c1[3] = event(c1[3])
    c2.append(hop(after(c2[1], clock)))
    twin("c13", c1[3])
    g1[2] = event(g1[2])
    g1.append(pop(g1[2]))
    g2.append(pop(after(g2[0], clock)))
    twin("g12", g1[2])
    lo_y = event(lo_y)
    hi_xy = event(hi_xy)
    lo_xy = event(lo_xy)
    xa = jnp.concatenate([n_lo, n_hi, lo_y, hi_y, lo_x, hi_x, lo_xy, hi_xy], axis=0)
    clock = xa
    d_far = send(after(d_nbr, clock), "y")
    c2[2] = event(c2[2])
    c2.append(hop(c2[2]))
    twin("c22", c2[2])
    g1[3] = event(g1[3])
    twin("g13", g1[3])
    g2[1] = event(g2[1])
    g2.append(pop(g2[1]))
    twin("g21", g2[1])

    def gate_up(at, own, far, part, rows_in):
        n = wide1 if at == 1 else wide2
        cols = slice(0, n) if at == 1 else slice(wide1, wide1 + n)
        wide = 2 * part + (LANES if at == 2 else 0)
        twins = [across[f"c{at}{s}"] for s in range(nz)] + [across[f"g{at}{s}"] for s in range(nz)]
        tile = lambda n: pl.BlockSpec((rows, n), lambda i: (i, 0))
        return call(
            functools.partial(gate_up_kernel, nz, blk, part),
            [((4 * rows, wide), BF16)],
            [rows_in, scale[:, cols], scale_oth[:, cols], *own, *far, *twins],
            in_specs=[tile(width), VM, VM] + [ANY] * (4 * nz),
            out_specs=[tile(wide)],
            grid=(4,),
            scratch_shapes=[
                pltpu.VMEM((width, 2 * n), BF16),
                pltpu.SemaphoreType.DMA((4 * nz,)),
            ],
            flops=4 * rows * width * n * 4,
            nbytes=4 * rows * (width + wide) * 2 + width * n * 4,
        )[0]

    h1 = gate_up(1, c1, g1, first, after(xa, clock))
    clock = h1
    c2[3] = event(c2[3])
    twin("c23", c2[3])
    g2[2] = event(g2[2])
    g2.append(pop(g2[2]))
    twin("g22", g2[2])
    d_far = event(d_far)
    even = [jnp.where(y == 0, d_own, d_far)]
    odd = [jnp.where(y == 0, d_far, d_own)]
    even.append(hop(even[0]))
    odd.append(pop(odd[0]))
    twin("e0", even[0])
    twin("o0", odd[0])
    g2[3] = event(g2[3])
    twin("g23", g2[3])
    h2 = gate_up(2, c2, g2, second, after(xa, clock))
    clock = h2

    cuts = ((0, first), (first, full), (full, quarter))

    def down(s):
        tile = lambda n: pl.BlockSpec((rows, n), lambda i: (i, 0))
        slot = lambda f: pl.BlockSpec((1, rows, blk), lambda i: (f(i), 0, 0))
        return call(
            functools.partial(down_kernel, cuts),
            [((2, rows, blk), BF16)] * 4,
            [after(h1, clock), h2, even[s], across[f"e{s}"], odd[s], across[f"o{s}"]],
            in_specs=[tile(h1.shape[1]), tile(h2.shape[1])] + [VM] * 4,
            out_specs=[
                slot(lambda i: jnp.minimum(i, 1)),
                slot(lambda i: jnp.maximum(i - 2, 0)),
                slot(lambda i: i // 2),
                slot(lambda i: i // 2),
            ],
            grid=(4,),
            scratch_shapes=[pltpu.VMEM((2 * quarter, 2 * blk), BF16)],
            flops=4 * rows * quarter * 8 * blk,
            nbytes=4 * rows * (2 * quarter + 2 * blk) * 2,
        )

    def second_add(*ins):
        one = pl.BlockSpec((1, rows, blk), lambda i: (1, 0, 0))
        whole = pl.BlockSpec((rows, blk), lambda i: (0, 0))
        return call(
            second_add_kernel,
            [((rows, blk), BF16)] * 2,
            list(ins),
            grid=(1,),
            in_specs=[one] * 4,
            out_specs=[whole] * 2,
            flops=4 * rows * blk,
            nbytes=2 * rows * blk * 6,
        )

    parts = []
    flying = None

    def land():
        nonlocal clock
        _, ax_keep, ax_got, ay_keep, ay_got = flying
        ax_got, ay_got = event(ax_got), event(ay_got)
        ax_next, ay_next = second_add(ax_keep, ax_got, ay_keep, ay_got)
        clock = ax_next
        parts.extend([ax_keep, ax_got, send(ax_next, "y")])
        parts.extend([ay_keep, ay_got, send(ay_next, "x")])

    for s in range(nz):
        ax_keep, ax_send, ay_keep, ay_send = down(s)
        clock = ax_keep
        now = (s, ax_keep, send(ax_send, "x"), ay_keep, send(ay_send, "y"))
        if s + 1 < nz:
            even[s + 1] = event(even[s + 1])
            odd[s + 1] = event(odd[s + 1])
            if s + 2 < nz:
                even.append(hop(even[s + 1]))
                odd.append(pop(odd[s + 1]))
            twin(f"e{s + 1}", even[s + 1])
            twin(f"o{s + 1}", odd[s + 1])
        if flying:
            land()
        flying = now
    land()

    third = pl.BlockSpec((1, lo, blk), lambda i: (0, i, 0))
    flat = pl.BlockSpec((lo, blk), lambda i: (i, 0))
    return call(
        functools.partial(final_kernel, nz, blk),
        [((rows, width), BF16)],
        [*parts, down_scale.reshape(1, -1)],
        grid=(rows // lo,),
        in_specs=[third, third, flat] * (2 * nz) + [VM],
        out_specs=[pl.BlockSpec((lo, width), lambda i: (i, 0))],
        flops=rows * width * 4,
        nbytes=rows * width * 8,
    )[0]


def solution(mesh):
    reps, shards, cores = (mesh.shape[a] for a in ("rep", "fs", "tp"))

    def run(*args):
        tokens, gate = args[0], args[2]
        rows = tokens.shape[0] // (reps * shards * cores)
        ffl, blk = gate.shape[1] // cores, gate.shape[0] // shards
        paired = (
            reps == 2
            and cores == 2
            and shards % 2 == 0
            and shards > 2
            and ffl % LANES == 0
            and ffl % (4 * LANES) == 2 * LANES
            and blk % LANES == 0
            and rows % 48 == 0
        )
        if paired:
            nz = shards // 2
            grid = Mesh(mesh.devices.reshape(reps, nz, 2, cores), ("x", "z", "y", "c"))
            row, deep, wide = ("x", "z", "y", "c"), ("z", "y"), "c"
            plan = functools.partial(pair_plan, nz)

            def body(*args):
                return plan(*args)

        else:
            grid, body = mesh, general_plan
            row, deep, wide = ("rep", "fs", "tp"), "fs", "tp"
        step = jax.shard_map(
            body,
            mesh=grid,
            in_specs=(
                P(row, None),
                P(),
                P(deep, wide),
                P(deep, wide),
                P(wide),
                P(wide),
                P(wide, deep),
                P(),
            ),
            out_specs=P(row, None),
            check_vma=False,
        )
        return step(*args)

    return run
```

time: 570 us -> 249 us (0.44)
  waiting for transfers between devices: 497 us -> 89.8 us
  Pallas kernels: 0 us -> 80.7 us
  starting transfers between devices: 0.17 us -> 53.4 us
  matrix products: 45.8 us -> 0 us
  local copies, waits for them, and re-layouts: 0.03 us -> 23.4 us
  other arithmetic: 13.6 us -> 0.05 us
  between operations: 13.2 us -> 0.65 us
    all_gather x4 -> x0, waiting for transfers between devices: 487 us -> none  [the longest x1 167 us: on_device(): lax.all_gather(gate_local, 'fs', axis=0, tiled=True)]
    ppermute x0 -> x68, waiting for transfers between devices: none -> 89.8 us  [send(): return lax.ppermute(v, axis, hops)]
    pallas_call x0 -> x15, Pallas kernels: none -> 80.7 us  [call(): pl.pallas_call(kernel, out_shape=[jax.ShapeDtypeStruct(s, d) for s, d in...]
    ppermute x0 -> x68, starting transfers between devices: none -> 53.4 us  [send(): return lax.ppermute(v, axis, hops)]
    dot_general x2 -> x0, matrix products: 45.8 us -> none  [the longest x1 30.1 us: on_device(): jnp.dot(hidden, lax.all_gather(down_weight.astype(jnp.bfloat16), 'fs', ax...]
    unnamed x12 -> x125, local copies, waits for them, and re-layouts: 0.03 us -> 18.7 us
    convert_element_type x5 -> x0, other arithmetic: 11.7 us -> none  [the longest x1 3.25 us: on_device(): down_weight.astype(jnp.bfloat16)]
    reduce_scatter x1 -> x0, waiting for transfers between devices: 9.51 us -> none  [on_device(): lax.psum_scatter(partial_value.astype(jnp.bfloat16), 'tp', scatter_dimens...]
  transfers between devices with their start and end apart: 5 -> 68, of which waited for: 5 -> 19; matrix products, arithmetic and copies ran while one was open for 4% -> 6% of each run, Pallas kernels for 0% -> 29%
where the time goes in v1:
time: 249 us; the launch traced here: 248 us
  waiting for transfers between devices  89.8 us (36%)
  Pallas kernels  80.7 us (32%)
  starting transfers between devices  53.4 us (21%)
  local copies, waits for them, and re-layouts  23.4 us (9%)
    ppermute x68, waiting for transfers between devices, send(): return lax.ppermute(v, axis, hops)  89.8 us
    pallas_call x15, Pallas kernels, call(): pl.pallas_call(kernel, out_shape=[jax.ShapeDtypeStruct(s, d) for s, d in...  80.7 us
    ppermute x68, starting transfers between devices, send(): return lax.ppermute(v, axis, hops)  53.4 us
    unnamed x125, local copies, waits for them, and re-layouts  18.7 us
  transfers between devices with their start and end apart: 68, of which 19 were waited for; matrix products, arithmetic and copies ran while one was open for 6% of the time, Pallas kernels for 29%

profile of v1, /device:TPU:0, one launch (start us, length us, event | category | flops | bytes accessed | tf_op | source)
XLA Modules:
  0.0 248.0 jit_solution(563800096321486035)
XLA Ops:
  0.0 3.9 %shard_map.82 = (bf16[256,1024]{1,0:T(8,128)(2,1)}, bf16[256,384]{1,0:T(8,128)(2,1)}, bf16[256,1024]{1,0:T(8,128)(2,1)}, bf16[256,384]{1,0:T(8,128)(2,1)}) custom-call(f32[256,2816]{1,0:T(8,128)} %g_ref.1, f32[256,2816]{1,0:T(8,128)} %u_ref.1), custom_call_target="tpu_custom_call" | custom-call | flops 1441792 | bytes 8650752 | tf_op jit(solution)/shard_map/pallas_call | solution.py:60
  3.9 3.0 %collective-permute-start.1 = (bf16[256,1024]{1,0:T(8,128)(2,1)}, bf16[256,1024]{1,0:T(8,128)(2,1)S(1)}, u32[]{:S(2)}, u32[]{:S(2)}) collective-permute-start(bf16[256,1024]{1,0:T(8,128)(2,1)} %get-tuple-element.93), channel_id=1, source_target_pairs={{0,2},{2,0},{1,3},{3,1},{4,6},{6,4},{5,7},{7,5},{8,10},{10,8},{9,1... | collective-permute-start | bytes 1572872 | tf_op jit(solution)/shard_map/ppermute | solution.py:235
  7.0 2.6 %collective-permute-start.2 = (bf16[256,1024]{1,0:T(8,128)(2,1)}, bf16[256,1024]{1,0:T(8,128)(2,1)S(1)}, u32[]{:S(2)}, u32[]{:S(2)}) collective-permute-start(bf16[256,1024]{1,0:T(8,128)(2,1)} %get-tuple-element.88.refs_0_), channel_id=1, source_target_pairs={{0,8},{8,12},{12,4},{4,0},{1,9},{9,13},{13,5},{5,1},{2,10},{10,14}... | collective-permute-start | bytes 1572872 | tf_op jit(solution)/shard_map/ppermute | solution.py:235
  9.5 3.0 %shard_map.83 = (bf16[128,2048]{1,0:T(8,128)(2,1)}, bf16[256,2048]{1,0:T(8,128)(2,1)}) custom-call(bf16[384,2048]{1,0:T(8,128)(2,1)} %t_ref, f32[1,2048]{1,0:T(1,128)} %bitcast.2), custom_call_target="tpu_custom_call" | custom-call | flops 6291456 | bytes 3145728 | tf_op jit(solution)/shard_map/pallas_call | solution.py:60
  12.5 1.5 collective-permute-start.5
  14.5 2.8 %shard_map.84 = (bf16[704,256]{1,0:T(8,128)(2,1)}, bf16[704,256]{1,0:T(8,128)(2,1)}) custom-call(f32[2816,256]{1,0:T(8,128)} %d_ref), custom_call_target="tpu_custom_call" | custom-call | flops 720896 | bytes 4325376 | tf_op jit(solution)/shard_map/pallas_call | solution.py:60
  17.3 3.5 %collective-permute-done.2.refs_1_ = bf16[256,1024]{1,0:T(8,128)(2,1)S(1)} collective-permute-done((bf16[256,1024]{1,0:T(8,128)(2,1)}, bf16[256,1024]{1,0:T(8,128)(2,1)S(1)}, u32[]{:S(2)}, u32[]{:S(2)}) %collective-permute-start.2) | collective-permute-done | bytes 524320 | tf_op jit(solution)/shard_map/ppermute | solution.py:235
  20.8 3.3 %collective-permute-start.6 = (bf16[256,1024]{1,0:T(8,128)(2,1)S(1)}, bf16[256,1024]{1,0:T(8,128)(2,1)}, u32[]{:S(2)}, u32[]{:S(2)}) collective-permute-start(bf16[256,1024]{1,0:T(8,128)(2,1)S(1)} %collective-permute-done.2.refs_1_), channel_id=1, source_target_pairs={{0,8},{8,12},{12,4},{4,0},{1,9},{9,13},{13,5},{5,1},{2,10},{10,14}... | collective-permute-start | bytes 1572872 | tf_op jit(solution)/shard_map/ppermute | solution.py:235
  24.1 2.9 %collective-permute-start = (bf16[256,384]{1,0:T(8,128)(2,1)}, bf16[256,384]{1,0:T(8,128)(2,1)S(1)}, u32[]{:S(2)}, u32[]{:S(2)}) collective-permute-start(bf16[256,384]{1,0:T(8,128)(2,1)} %get-tuple-element.92.refs_0_), channel_id=1, source_target_pairs={{0,8},{8,12},{12,4},{4,0},{1,9},{9,13},{13,5},{5,1},{2,10},{10,14}... | collective-permute-start | bytes 589832 | tf_op jit(solution)/shard_map/ppermute | solution.py:235
  27.0 22.7 %collective-permute-done.refs_1_ = bf16[256,384]{1,0:T(8,128)(2,1)S(1)} collective-permute-done((bf16[256,384]{1,0:T(8,128)(2,1)}, bf16[256,384]{1,0:T(8,128)(2,1)S(1)}, u32[]{:S(2)}, u32[]{:S(2)}) %collective-permute-start) | collective-permute-done | bytes 196640 | tf_op jit(solution)/shard_map/ppermute | solution.py:235
  49.7 1.5 collective-permute-start.10
  51.2 3.3 %collective-permute-start.8 = (bf16[256,1024]{1,0:T(8,128)(2,1)}, bf16[256,1024]{1,0:T(8,128)(2,1)}, u32[]{:S(2)}, u32[]{:S(2)}) collective-permute-start(bf16[256,1024]{1,0:T(8,128)(2,1)} %collective-permute-done.6.refs_2_), channel_id=1, source_target_pairs={{0,8},{8,12},{12,4},{4,0},{1,9},{9,13},{13,5},{5,1},{2,10},{10,14}... | collective-permute-start | bytes 1572872 | tf_op jit(solution)/shard_map/ppermute | solution.py:235
  56.9 1.9 constant_dynamic-update-slice_fusion.7
  58.8 1.4 shard_map.85
  60.2 4.6 %collective-permute-done.10 = bf16[128,2048]{1,0:T(8,128)(2,1)} collective-permute-done((bf16[128,2048]{1,0:T(8,128)(2,1)}, bf16[128,2048]{1,0:T(8,128)(2,1)}, u32[]{:S(2)}, u32[]{:S(2)}) %collective-permute-start.10) | collective-permute-done | bytes 524320 | tf_op jit(solution)/shard_map/ppermute | solution.py:235
  65.3 2.3 constant_dynamic-update-slice_fusion.6
  67.6 3.1 %collective-permute-done.9.refs_4_ = bf16[256,384]{1,0:T(8,128)(2,1)S(1)} collective-permute-done((bf16[256,384]{1,0:T(8,128)(2,1)}, bf16[256,384]{1,0:T(8,128)(2,1)S(1)}, u32[]{:S(2)}, u32[]{:S(2)}) %collective-permute-start.9) | collective-permute-done | bytes 196640 | tf_op jit(solution)/shard_map/ppermute | solution.py:235
  71.2 5.2 %collective-permute-done.7.refs_6_ = bf16[256,1024]{1,0:T(8,128)(2,1)} collective-permute-done((bf16[256,1024]{1,0:T(8,128)(2,1)}, bf16[256,1024]{1,0:T(8,128)(2,1)}, u32[]{:S(2)}, u32[]{:S(2)}) %collective-permute-start.7) | collective-permute-done | bytes 524320 | tf_op jit(solution)/shard_map/ppermute | solution.py:235
  77.7 1.9 constant_dynamic-update-slice_fusion.5
  79.6 1.0 constant_dynamic-update-slice_fusion.4
  80.6 1.9 constant_dynamic-update-slice_fusion.3
  82.5 1.6 collective-permute-done.13
  84.1 1.1 constant_dynamic-update-slice_fusion.2
  85.2 5.3 %collective-permute-done.12 = bf16[128,2048]{1,0:T(8,128)(2,1)S(1)} collective-permute-done((bf16[128,2048]{1,0:T(8,128)(2,1)}, bf16[128,2048]{1,0:T(8,128)(2,1)S(1)}, u32[]{:S(2)}, u32[]{:S(2)}) %collective-permute-start.12) | collective-permute-done | bytes 524320 | tf_op jit(solution)/shard_map/ppermute | solution.py:235
  90.5 0.8 constant_dynamic-update-slice_fusion.1
  91.3 5.2 %collective-permute-done.16.refs_2_ = bf16[256,384]{1,0:T(8,128)(2,1)} collective-permute-done((bf16[256,384]{1,0:T(8,128)(2,1)S(1)}, bf16[256,384]{1,0:T(8,128)(2,1)}, u32[]{:S(2)}, u32[]{:S(2)}) %collective-permute-start.16) | collective-permute-done | bytes 196640 | tf_op jit(solution)/shard_map/ppermute | solution.py:235
  96.6 1.4 collective-permute-start.14
  98.0 1.1 constant_dynamic-update-slice_fusion.x_ref
  100.1 4.8 %collective-permute-done.14.refs_5_ = bf16[256,384]{1,0:T(8,128)(2,1)} collective-permute-done((bf16[256,384]{1,0:T(8,128)(2,1)S(1)}, bf16[256,384]{1,0:T(8,128)(2,1)}, u32[]{:S(2)}, u32[]{:S(2)}) %collective-permute-start.14) | collective-permute-done | bytes 196640 | tf_op jit(solution)/shard_map/ppermute | solution.py:235
  106.6 2.5 %collective-permute-start.27 = (bf16[256,384]{1,0:T(8,128)(2,1)}, bf16[256,384]{1,0:T(8,128)(2,1)}, u32[]{:S(2)}, u32[]{:S(2)}) collective-permute-start(bf16[256,384]{1,0:T(8,128)(2,1)} %collective-permute-done.16.refs_2_), channel_id=1, source_target_pairs={{0,8},{8,12},{12,4},{4,0},{1,9},{9,13},{13,5},{5,1},{2,10},{10,14}... | collective-permute-start | bytes 589832 | tf_op jit(solution)/shard_map/ppermute | solution.py:235
  109.1 1.0 collective-permute-start.29
  110.9 19.8 %shard_map.86.h1 = bf16[1536,1024]{1,0:T(8,128)(2,1)} custom-call(bf16[1536,2048]{1,0:T(8,128)(2,1)} %constant_dynamic-update-slice_fusion.x_ref, f32[1,1024]{1,0:T(1,128)} %slice.16.s_own, f32[1,1024]{1,0:T(1,128)} %slice.17.s_oth, bf16[256,1024]{1,0:T(8,128)(2,1)} %get-tuple-element.88.refs_0_, bf16[256,1024]{1,0:T(8,128)(2,1)} %copy-done.24, ...), custom_call_target="tpu_custom_call" | custom-call | flops 12884901888 | bytes 17825792 | tf_op jit(solution)/shard_map/pallas_call | solution.py:60
  133.5 4.9 %collective-permute-done.28.refs_7_ = bf16[256,384]{1,0:T(8,128)(2,1)S(1)} collective-permute-done((bf16[256,384]{1,0:T(8,128)(2,1)}, bf16[256,384]{1,0:T(8,128)(2,1)S(1)}, u32[]{:S(2)}, u32[]{:S(2)}) %collective-permute-start.28) | collective-permute-done | bytes 196640 | tf_op jit(solution)/shard_map/ppermute | solution.py:235
  141.2 2.4 collective-permute-start.42
  143.7 10.6 %shard_map.87.h2 = bf16[1536,384]{1,0:T(8,128)(2,1)} custom-call(bf16[1536,2048]{1,0:T(8,128)(2,1)} %constant_dynamic-update-slice_fusion.x_ref, f32[1,384]{1,0:T(1,128)} %slice.18.s_own, f32[1,384]{1,0:T(1,128)} %slice.19.s_oth, bf16[256,384]{1,0:T(8,128)(2,1)} %get-tuple-element.92.refs_0_, bf16[256,384]{1,0:T(8,128)(2,1)} %copy-done.48, ...), custom_call_target="tpu_custom_call" | custom-call | flops 4831838208 | bytes 10616832 | tf_op jit(solution)/shard_map/pallas_call | solution.py:60
  155.9 6.6 %shard_map.88 = (bf16[2,384,256]{2,1,0:T(8,128)(2,1)}, bf16[2,384,256]{2,1,0:T(8,128)(2,1)}, bf16[2,384,256]{2,1,0:T(8,128)(2,1)}, bf16[2,384,256]{2,1,0:T(8,128)(2,1)}) custom-call(bf16[1536,1024]{1,0:T(8,128)(2,1)} %shard_map.86.h1, bf16[1536,384]{1,0:T(8,128)(2,1)} %shard_map.87.h2, bf16[704,256]{1,0:T(8,128)(2,1)} %copy-done.10, ...), custom_call_target="tpu_custom_call" | custom-call | flops 2214592512 | bytes 5898240 | tf_op jit(solution)/shard_map/pallas_call | solution.py:60
  163.1 1.0 collective-permute-start.44
  164.1 1.0 collective-permute-start.43
  165.7 1.1 collective-permute-start.47
  167.6 6.6 %shard_map.89 = (bf16[2,384,256]{2,1,0:T(8,128)(2,1)}, bf16[2,384,256]{2,1,0:T(8,128)(2,1)}, bf16[2,384,256]{2,1,0:T(8,128)(2,1)}, bf16[2,384,256]{2,1,0:T(8,128)(2,1)}) custom-call(bf16[1536,1024]{1,0:T(8,128)(2,1)} %shard_map.86.h1, bf16[1536,384]{1,0:T(8,128)(2,1)} %shard_map.87.h2, bf16[704,256]{1,0:T(8,128)(2,1)} %copy-done.38, ...), custom_call_target="tpu_custom_call" | custom-call | flops 2214592512 | bytes 5898240 | tf_op jit(solution)/shard_map/pallas_call | solution.py:60
  174.3 8.2 %collective-permute-done.43.b_own = bf16[704,256]{1,0:T(8,128)(2,1)S(1)} collective-permute-done((bf16[704,256]{1,0:T(8,128)(2,1)S(1)}, bf16[704,256]{1,0:T(8,128)(2,1)S(1)}, u32[]{:S(2)}, u32[]{:S(2)}) %collective-permute-start.43) | collective-permute-done | bytes 360480 | tf_op jit(solution)/shard_map/ppermute | solution.py:235
  183.1 1.4 collective-permute-start.51
  185.3 2.0 shard_map.90
  188.1 0.8 collective-permute-start.55
  188.9 6.7 %shard_map.91 = (bf16[2,384,256]{2,1,0:T(8,128)(2,1)}, bf16[2,384,256]{2,1,0:T(8,128)(2,1)}, bf16[2,384,256]{2,1,0:T(8,128)(2,1)}, bf16[2,384,256]{2,1,0:T(8,128)(2,1)}) custom-call(bf16[1536,1024]{1,0:T(8,128)(2,1)} %shard_map.86.h1, bf16[1536,384]{1,0:T(8,128)(2,1)} %shard_map.87.h2, bf16[704,256]{1,0:T(8,128)(2,1)} %copy-done.37, ...), custom_call_target="tpu_custom_call" | custom-call | flops 2214592512 | bytes 5898240 | tf_op jit(solution)/shard_map/pallas_call | solution.py:60
  195.7 5.4 %collective-permute-done.51.b_own = bf16[704,256]{1,0:T(8,128)(2,1)S(1)} collective-permute-done((bf16[704,256]{1,0:T(8,128)(2,1)S(1)}, bf16[704,256]{1,0:T(8,128)(2,1)S(1)}, u32[]{:S(2)}, u32[]{:S(2)}) %collective-permute-start.51) | collective-permute-done | bytes 360480 | tf_op jit(solution)/shard_map/ppermute | solution.py:235
  201.7 0.8 collective-permute-start.61
  203.3 2.0 shard_map.92
  206.8 6.7 %shard_map.93 = (bf16[2,384,256]{2,1,0:T(8,128)(2,1)}, bf16[2,384,256]{2,1,0:T(8,128)(2,1)}, bf16[2,384,256]{2,1,0:T(8,128)(2,1)}, bf16[2,384,256]{2,1,0:T(8,128)(2,1)}) custom-call(bf16[1536,1024]{1,0:T(8,128)(2,1)} %shard_map.86.h1, bf16[1536,384]{1,0:T(8,128)(2,1)} %shard_map.87.h2, bf16[704,256]{1,0:T(8,128)(2,1)} %copy-done.36, ...), custom_call_target="tpu_custom_call" | custom-call | flops 2214592512 | bytes 5898240 | tf_op jit(solution)/shard_map/pallas_call | solution.py:60
  213.5 1.5 collective-permute-start.64
  215.0 1.2 collective-permute-start.65
  216.2 0.8 collective-permute-start.48
  217.6 1.2 collective-permute-start.56
  218.9 2.0 shard_map.94
  220.9 4.8 %collective-permute-done.64.ax_got.refs_19_ = bf16[2,384,256]{2,1,0:T(8,128)(2,1)S(1)} collective-permute-done((bf16[2,384,256]{2,1,0:T(8,128)(2,1)}, bf16[2,384,256]{2,1,0:T(8,128)(2,1)S(1)}, u32[]{:S(2)}, u32[]{:S(2)}) %collective-permute-start.64) | collective-permute-done | bytes 393248 | tf_op jit(solution)/shard_map/ppermute | solution.py:235
  225.7 1.5 collective-permute-start.57
  227.2 1.2 collective-permute-start.62
  228.4 2.0 shard_map.95
  230.5 1.0 collective-permute-done.48.refs_2_
  231.9 1.2 collective-permute-start.66
  233.2 2.5 collective-permute-done.56.refs_8_
  236.2 3.7 %collective-permute-done.62.refs_14_ = bf16[384,256]{1,0:T(8,128)(2,1)S(1)} collective-permute-done((bf16[384,256]{1,0:T(8,128)(2,1)}, bf16[384,256]{1,0:T(8,128)(2,1)S(1)}, u32[]{:S(2)}, u32[]{:S(2)}) %collective-permute-start.62) | collective-permute-done | bytes 196640 | tf_op jit(solution)/shard_map/ppermute | solution.py:235
  239.8 2.9 %collective-permute-done.66.refs_20_ = bf16[384,256]{1,0:T(8,128)(2,1)S(1)} collective-permute-done((bf16[384,256]{1,0:T(8,128)(2,1)}, bf16[384,256]{1,0:T(8,128)(2,1)S(1)}, u32[]{:S(2)}, u32[]{:S(2)}) %collective-permute-start.66) | collective-permute-done | bytes 196640 | tf_op jit(solution)/shard_map/ppermute | solution.py:235
  243.5 4.4 %shard_map.96 = bf16[384,2048]{1,0:T(8,128)(2,1)} custom-call(bf16[2,384,256]{2,1,0:T(8,128)(2,1)} %get-tuple-element.130.ax_keep.refs_0_, bf16[2,384,256]{2,1,0:T(8,128)(2,1)} %copy-done, bf16[384,256]{1,0:T(8,128)(2,1)} %copy-done.11, bf16[2,384,256]{2,1,0:T(8,128)(2,1)} %get-tuple-element.139.ay_keep.refs_3_, bf16[2,384,256]{2,1,0:T(8,128)(2,1)} %copy-done.1, ...), custom_call_target="tpu_custom_call" | custom-call | flops 3145728 | bytes 6291456 | tf_op jit(solution)/shard_map/pallas_call | solution.py:60
  (220 shorter events, 25.3 us)
Async XLA Ops:
  3.9 20.1 %collective-permute-start.1 = (bf16[256,1024]{1,0:T(8,128)(2,1)}, bf16[256,1024]{1,0:T(8,128)(2,1)S(1)}, u32[]{:S(2)}, u32[]{:S(2)}) collective-permute-start(bf16[256,1024]{1,0:T(8,128)(2,1)} %get-tuple-element.93), channel_id=1, source_target_pairs={{0,2},{2,0},{1,3},{3,1},{4,6},{6,4},{5,7},{7,5},{8,10},{10,8},{9,1... | collective-permute-start | bytes 1572872 | tf_op jit(solution)/shard_map/ppermute | solution.py:235
  7.0 13.8 %collective-permute-start.2 = (bf16[256,1024]{1,0:T(8,128)(2,1)}, bf16[256,1024]{1,0:T(8,128)(2,1)S(1)}, u32[]{:S(2)}, u32[]{:S(2)}) collective-permute-start(bf16[256,1024]{1,0:T(8,128)(2,1)} %get-tuple-element.88.refs_0_), channel_id=1, source_target_pairs={{0,8},{8,12},{12,4},{4,0},{1,9},{9,13},{13,5},{5,1},{2,10},{10,14}... | collective-permute-start | bytes 1572872 | tf_op jit(solution)/shard_map/ppermute | solution.py:235
  12.5 41.9 %collective-permute-start.5 = (bf16[256,2048]{1,0:T(8,128)(2,1)}, bf16[256,2048]{1,0:T(8,128)(2,1)S(1)}, u32[]{:S(2)}, u32[]{:S(2)}) collective-permute-start(bf16[256,2048]{1,0:T(8,128)(2,1)} %get-tuple-element.91), channel_id=1, source_target_pairs={{0,16},{16,0},{1,17},{17,1},{2,18},{18,2},{3,19},{19,3},{4,20},{20... | collective-permute-start | bytes 3145736 | tf_op jit(solution)/shard_map/ppermute | solution.py:235
  14.0 42.3 %collective-permute-start.11 = (bf16[256,2048]{1,0:T(8,128)(2,1)}, bf16[256,2048]{1,0:T(8,128)(2,1)S(1)}, u32[]{:S(2)}, u32[]{:S(2)}) collective-permute-start(bf16[256,2048]{1,0:T(8,128)(2,1)} %get-tuple-element.91), channel_id=1, source_target_pairs={{0,2},{2,0},{1,3},{3,1},{4,6},{6,4},{5,7},{7,5},{8,10},{10,8},{9,1... | collective-permute-start | bytes 3145736 | tf_op jit(solution)/shard_map/ppermute | solution.py:235
  20.8 30.4 %collective-permute-start.6 = (bf16[256,1024]{1,0:T(8,128)(2,1)S(1)}, bf16[256,1024]{1,0:T(8,128)(2,1)}, u32[]{:S(2)}, u32[]{:S(2)}) collective-permute-start(bf16[256,1024]{1,0:T(8,128)(2,1)S(1)} %collective-permute-done.2.refs_1_), channel_id=1, source_target_pairs={{0,8},{8,12},{12,4},{4,0},{1,9},{9,13},{13,5},{5,1},{2,10},{10,14}... | collective-permute-start | bytes 1572872 | tf_op jit(solution)/shard_map/ppermute | solution.py:235
  24.0 30.4 %collective-permute-start.4 = (bf16[256,1024]{1,0:T(8,128)(2,1)S(1)}, bf16[256,1024]{1,0:T(8,128)(2,1)}, u32[]{:S(2)}, u32[]{:S(2)}) collective-permute-start(bf16[256,1024]{1,0:T(8,128)(2,1)S(1)} %collective-permute-done.1.refs_4_), channel_id=1, source_target_pairs={{8,0},{12,8},{4,12},{0,4},{9,1},{13,9},{5,13},{1,5},{10,2},{14,10}... | collective-permute-start | bytes 1572872 | tf_op jit(solution)/shard_map/ppermute | solution.py:235
  24.1 25.6 %collective-permute-start = (bf16[256,384]{1,0:T(8,128)(2,1)}, bf16[256,384]{1,0:T(8,128)(2,1)S(1)}, u32[]{:S(2)}, u32[]{:S(2)}) collective-permute-start(bf16[256,384]{1,0:T(8,128)(2,1)} %get-tuple-element.92.refs_0_), channel_id=1, source_target_pairs={{0,8},{8,12},{12,4},{4,0},{1,9},{9,13},{13,5},{5,1},{2,10},{10,14}... | collective-permute-start | bytes 589832 | tf_op jit(solution)/shard_map/ppermute | solution.py:235
  49.7 15.1 %collective-permute-start.10 = (bf16[128,2048]{1,0:T(8,128)(2,1)}, bf16[128,2048]{1,0:T(8,128)(2,1)}, u32[]{:S(2)}, u32[]{:S(2)}) collective-permute-start(bf16[128,2048]{1,0:T(8,128)(2,1)} %get-tuple-element.105), channel_id=1, source_target_pairs={{0,16},{16,0},{1,17},{17,1},{2,18},{18,2},{3,19},{19,3},{4,20},{20... | collective-permute-start | bytes 1572872 | tf_op jit(solution)/shard_map/ppermute | solution.py:235
  51.2 19.5 %collective-permute-start.8 = (bf16[256,1024]{1,0:T(8,128)(2,1)}, bf16[256,1024]{1,0:T(8,128)(2,1)}, u32[]{:S(2)}, u32[]{:S(2)}) collective-permute-start(bf16[256,1024]{1,0:T(8,128)(2,1)} %collective-permute-done.6.refs_2_), channel_id=1, source_target_pairs={{0,8},{8,12},{12,4},{4,0},{1,9},{9,13},{13,5},{5,1},{2,10},{10,14}... | collective-permute-start | bytes 1572872 | tf_op jit(solution)/shard_map/ppermute | solution.py:235
  54.5 22.0 %collective-permute-start.7 = (bf16[256,1024]{1,0:T(8,128)(2,1)}, bf16[256,1024]{1,0:T(8,128)(2,1)}, u32[]{:S(2)}, u32[]{:S(2)}) collective-permute-start(bf16[256,1024]{1,0:T(8,128)(2,1)} %collective-permute-done.4.refs_5_), channel_id=1, source_target_pairs={{8,0},{12,8},{4,12},{0,4},{9,1},{13,9},{5,13},{1,5},{10,2},{14,10}... | collective-permute-start | bytes 1572872 | tf_op jit(solution)/shard_map/ppermute | solution.py:235
  54.5 22.4 %collective-permute-start.3 = (bf16[128,2048]{1,0:T(8,128)(2,1)}, bf16[128,2048]{1,0:T(8,128)(2,1)}, u32[]{:S(2)}, u32[]{:S(2)}) collective-permute-start(bf16[128,2048]{1,0:T(8,128)(2,1)} %get-tuple-element.105), channel_id=1, source_target_pairs={{0,2},{2,0},{1,3},{3,1},{4,6},{6,4},{5,7},{7,5},{8,10},{10,8},{9,1... | collective-permute-start | bytes 1572872 | tf_op jit(solution)/shard_map/ppermute | solution.py:235
  56.3 27.7 %collective-permute-start.13 = (bf16[256,2048]{1,0:T(8,128)(2,1)S(1)}, bf16[256,2048]{1,0:T(8,128)(2,1)S(1)}, u32[]{:S(2)}, u32[]{:S(2)}) collective-permute-start(bf16[256,2048]{1,0:T(8,128)(2,1)S(1)} %collective-permute-done.11), channel_id=1, source_target_pairs={{0,16},{16,0},{1,17},{17,1},{2,18},{18,2},{3,19},{19,3},{4,20},{20... | collective-permute-start | bytes 3145736 | tf_op jit(solution)/shard_map/ppermute | solution.py:235
  64.8 5.9 %collective-permute-start.9 = (bf16[256,384]{1,0:T(8,128)(2,1)}, bf16[256,384]{1,0:T(8,128)(2,1)S(1)}, u32[]{:S(2)}, u32[]{:S(2)}) collective-permute-start(bf16[256,384]{1,0:T(8,128)(2,1)} %get-tuple-element.104), channel_id=1, source_target_pairs={{0,2},{2,0},{1,3},{3,1},{4,6},{6,4},{5,7},{7,5},{8,10},{10,8},{9,1... | collective-permute-start | bytes 589832 | tf_op jit(solution)/shard_map/ppermute | solution.py:235
  70.7 28.6 %collective-permute-start.18 = (bf16[256,1024]{1,0:T(8,128)(2,1)}, bf16[256,1024]{1,0:T(8,128)(2,1)S(1)}, u32[]{:S(2)}, u32[]{:S(2)}) collective-permute-start(bf16[256,1024]{1,0:T(8,128)(2,1)} %get-tuple-element.88.refs_0_), channel_id=1, source_target_pairs={{0,1},{1,0},{2,3},{3,2},{4,5},{5,4},{6,7},{7,6},{8,9},{9,8},{10,11... | collective-permute-start | bytes 1572872 | tf_op jit(solution)/shard_map/ppermute | solution.py:235
  70.7 28.9 %collective-permute-start.19 = (bf16[256,1024]{1,0:T(8,128)(2,1)}, bf16[256,1024]{1,0:T(8,128)(2,1)S(1)}, u32[]{:S(2)}, u32[]{:S(2)}) collective-permute-start(bf16[256,1024]{1,0:T(8,128)(2,1)} %copy-done.24), channel_id=1, source_target_pairs={{0,1},{1,0},{2,3},{3,2},{4,5},{5,4},{6,7},{7,6},{8,9},{9,8},{10,11... | collective-permute-start | bytes 1572872 | tf_op jit(solution)/shard_map/ppermute | solution.py:235
  76.4 14.1 %collective-permute-start.12 = (bf16[128,2048]{1,0:T(8,128)(2,1)}, bf16[128,2048]{1,0:T(8,128)(2,1)S(1)}, u32[]{:S(2)}, u32[]{:S(2)}) collective-permute-start(bf16[128,2048]{1,0:T(8,128)(2,1)} %collective-permute-done.10), channel_id=1, source_target_pairs={{0,2},{2,0},{1,3},{3,1},{4,6},{6,4},{5,7},{7,5},{8,10},{10,8},{9,1... | collective-permute-start | bytes 1572872 | tf_op jit(solution)/shard_map/ppermute | solution.py:235
  76.9 19.6 %collective-permute-start.15 = (bf16[256,1024]{1,0:T(8,128)(2,1)}, bf16[256,1024]{1,0:T(8,128)(2,1)S(1)}, u32[]{:S(2)}, u32[]{:S(2)}) collective-permute-start(bf16[256,1024]{1,0:T(8,128)(2,1)} %collective-permute-done.7.refs_6_), channel_id=1, source_target_pairs={{8,0},{12,8},{4,12},{0,4},{9,1},{13,9},{5,13},{1,5},{10,2},{14,10}... | collective-permute-start | bytes 1572872 | tf_op jit(solution)/shard_map/ppermute | solution.py:235
  84.1 15.7 %collective-permute-start.22 = (bf16[256,1024]{1,0:T(8,128)(2,1)S(1)}, bf16[256,1024]{1,0:T(8,128)(2,1)S(1)}, u32[]{:S(2)}, u32[]{:S(2)}) collective-permute-start(bf16[256,1024]{1,0:T(8,128)(2,1)S(1)} %copy-done.23), channel_id=1, source_target_pairs={{0,1},{1,0},{2,3},{3,2},{4,5},{5,4},{6,7},{7,6},{8,9},{9,8},{10,11... | collective-permute-start | bytes 1572872 | tf_op jit(solution)/shard_map/ppermute | solution.py:235
  90.5 6.1 %collective-permute-start.16 = (bf16[256,384]{1,0:T(8,128)(2,1)S(1)}, bf16[256,384]{1,0:T(8,128)(2,1)}, u32[]{:S(2)}, u32[]{:S(2)}) collective-permute-start(bf16[256,384]{1,0:T(8,128)(2,1)S(1)} %copy-done.49), channel_id=1, source_target_pairs={{0,8},{8,12},{12,4},{4,0},{1,9},{9,13},{13,5},{5,1},{2,10},{10,14}... | collective-permute-start | bytes 589832 | tf_op jit(solution)/shard_map/ppermute | solution.py:235
  96.6 8.3 %collective-permute-start.14 = (bf16[256,384]{1,0:T(8,128)(2,1)S(1)}, bf16[256,384]{1,0:T(8,128)(2,1)}, u32[]{:S(2)}, u32[]{:S(2)}) collective-permute-start(bf16[256,384]{1,0:T(8,128)(2,1)S(1)} %collective-permute-done.9.refs_4_), channel_id=1, source_target_pairs={{8,0},{12,8},{4,12},{0,4},{9,1},{13,9},{5,13},{1,5},{10,2},{14,10}... | collective-permute-start | bytes 589832 | tf_op jit(solution)/shard_map/ppermute | solution.py:235
  99.1 7.0 %collective-permute-start.20 = (bf16[256,1024]{1,0:T(8,128)(2,1)}, bf16[256,1024]{1,0:T(8,128)(2,1)S(1)}, u32[]{:S(2)}, u32[]{:S(2)}) collective-permute-start(bf16[256,1024]{1,0:T(8,128)(2,1)} %collective-permute-done.6.refs_2_), channel_id=1, source_target_pairs={{0,1},{1,0},{2,3},{3,2},{4,5},{5,4},{6,7},{7,6},{8,9},{9,8},{10,11... | collective-permute-start | bytes 1572872 | tf_op jit(solution)/shard_map/ppermute | solution.py:235
  99.2 7.4 %collective-permute-start.23 = (bf16[256,1024]{1,0:T(8,128)(2,1)}, bf16[256,1024]{1,0:T(8,128)(2,1)S(1)}, u32[]{:S(2)}, u32[]{:S(2)}) collective-permute-start(bf16[256,1024]{1,0:T(8,128)(2,1)} %collective-permute-done.4.refs_5_), channel_id=1, source_target_pairs={{0,1},{1,0},{2,3},{3,2},{4,5},{5,4},{6,7},{7,6},{8,9},{9,8},{10,11... | collective-permute-start | bytes 1572872 | tf_op jit(solution)/shard_map/ppermute | solution.py:235
  99.6 9.5 %collective-permute-start.21 = (bf16[256,1024]{1,0:T(8,128)(2,1)}, bf16[256,1024]{1,0:T(8,128)(2,1)S(1)}, u32[]{:S(2)}, u32[]{:S(2)}) collective-permute-start(bf16[256,1024]{1,0:T(8,128)(2,1)} %collective-permute-done.8.refs_3_), channel_id=1, source_target_pairs={{0,1},{1,0},{2,3},{3,2},{4,5},{5,4},{6,7},{7,6},{8,9},{9,8},{10,11... | collective-permute-start | bytes 1572872 | tf_op jit(solution)/shard_map/ppermute | solution.py:235
  99.8 10.3 %collective-permute-start.24 = (bf16[256,1024]{1,0:T(8,128)(2,1)}, bf16[256,1024]{1,0:T(8,128)(2,1)S(1)}, u32[]{:S(2)}, u32[]{:S(2)}) collective-permute-start(bf16[256,1024]{1,0:T(8,128)(2,1)} %collective-permute-done.7.refs_6_), channel_id=1, source_target_pairs={{0,1},{1,0},{2,3},{3,2},{4,5},{5,4},{6,7},{7,6},{8,9},{9,8},{10,11... | collective-permute-start | bytes 1572872 | tf_op jit(solution)/shard_map/ppermute | solution.py:235
  104.9 6.0 %collective-permute-start.25 = (bf16[256,1024]{1,0:T(8,128)(2,1)S(1)}, bf16[256,1024]{1,0:T(8,128)(2,1)}, u32[]{:S(2)}, u32[]{:S(2)}) collective-permute-start(bf16[256,1024]{1,0:T(8,128)(2,1)S(1)} %collective-permute-done.15.refs_7_), channel_id=1, source_target_pairs={{0,1},{1,0},{2,3},{3,2},{4,5},{5,4},{6,7},{7,6},{8,9},{9,8},{10,11... | collective-permute-start | bytes 1572872 | tf_op jit(solution)/shard_map/ppermute | solution.py:235
  106.1 24.7 %collective-permute-start.26 = (bf16[256,384]{1,0:T(8,128)(2,1)}, bf16[256,384]{1,0:T(8,128)(2,1)}, u32[]{:S(2)}, u32[]{:S(2)}) collective-permute-start(bf16[256,384]{1,0:T(8,128)(2,1)} %collective-permute-done.14.refs_5_), channel_id=1, source_target_pairs={{8,0},{12,8},{4,12},{0,4},{9,1},{13,9},{5,13},{1,5},{10,2},{14,10}... | collective-permute-start | bytes 589832 | tf_op jit(solution)/shard_map/ppermute | solution.py:235
  106.6 24.2 %collective-permute-start.27 = (bf16[256,384]{1,0:T(8,128)(2,1)}, bf16[256,384]{1,0:T(8,128)(2,1)}, u32[]{:S(2)}, u32[]{:S(2)}) collective-permute-start(bf16[256,384]{1,0:T(8,128)(2,1)} %collective-permute-done.16.refs_2_), channel_id=1, source_target_pairs={{0,8},{8,12},{12,4},{4,0},{1,9},{9,13},{13,5},{5,1},{2,10},{10,14}... | collective-permute-start | bytes 589832 | tf_op jit(solution)/shard_map/ppermute | solution.py:235
  109.1 23.9 %collective-permute-start.29 = (bf16[704,256]{1,0:T(8,128)(2,1)S(1)}, bf16[704,256]{1,0:T(8,128)(2,1)S(1)}, u32[]{:S(2)}, u32[]{:S(2)}) collective-permute-start(bf16[704,256]{1,0:T(8,128)(2,1)S(1)} %copy-done.33), channel_id=1, source_target_pairs={{0,2},{2,0},{1,3},{3,1},{4,6},{6,4},{5,7},{7,5},{8,10},{10,8},{9,1... | collective-permute-start | bytes 1081352 | tf_op jit(solution)/shard_map/ppermute | solution.py:235
  130.8 7.6 %collective-permute-start.28 = (bf16[256,384]{1,0:T(8,128)(2,1)}, bf16[256,384]{1,0:T(8,128)(2,1)S(1)}, u32[]{:S(2)}, u32[]{:S(2)}) collective-permute-start(bf16[256,384]{1,0:T(8,128)(2,1)} %collective-permute-done.26.refs_6_), channel_id=1, source_target_pairs={{8,0},{12,8},{4,12},{0,4},{9,1},{13,9},{5,13},{1,5},{10,2},{14,10}... | collective-permute-start | bytes 589832 | tf_op jit(solution)/shard_map/ppermute | solution.py:235
  131.3 7.1 %collective-permute-start.30 = (bf16[256,384]{1,0:T(8,128)(2,1)S(1)}, bf16[256,384]{1,0:T(8,128)(2,1)S(1)}, u32[]{:S(2)}, u32[]{:S(2)}) collective-permute-start(bf16[256,384]{1,0:T(8,128)(2,1)S(1)} %copy-done.47), channel_id=1, source_target_pairs={{0,1},{1,0},{2,3},{3,2},{4,5},{5,4},{6,7},{7,6},{8,9},{9,8},{10,11... | collective-permute-start | bytes 589832 | tf_op jit(solution)/shard_map/ppermute | solution.py:235
  131.3 7.6 %collective-permute-start.31 = (bf16[256,384]{1,0:T(8,128)(2,1)}, bf16[256,384]{1,0:T(8,128)(2,1)S(1)}, u32[]{:S(2)}, u32[]{:S(2)}) collective-permute-start(bf16[256,384]{1,0:T(8,128)(2,1)} %copy-done.48), channel_id=1, source_target_pairs={{0,1},{1,0},{2,3},{3,2},{4,5},{5,4},{6,7},{7,6},{8,9},{9,8},{10,11... | collective-permute-start | bytes 589832 | tf_op jit(solution)/shard_map/ppermute | solution.py:235
  131.8 7.2 %collective-permute-start.34 = (bf16[256,384]{1,0:T(8,128)(2,1)}, bf16[256,384]{1,0:T(8,128)(2,1)S(1)}, u32[]{:S(2)}, u32[]{:S(2)}) collective-permute-start(bf16[256,384]{1,0:T(8,128)(2,1)} %copy-done.50), channel_id=1, source_target_pairs={{0,1},{1,0},{2,3},{3,2},{4,5},{5,4},{6,7},{7,6},{8,9},{9,8},{10,11... | collective-permute-start | bytes 589832 | tf_op jit(solution)/shard_map/ppermute | solution.py:235
  133.0 6.5 %collective-permute-start.32 = (bf16[256,384]{1,0:T(8,128)(2,1)}, bf16[256,384]{1,0:T(8,128)(2,1)S(1)}, u32[]{:S(2)}, u32[]{:S(2)}) collective-permute-start(bf16[256,384]{1,0:T(8,128)(2,1)} %collective-permute-done.16.refs_2_), channel_id=1, source_target_pairs={{0,1},{1,0},{2,3},{3,2},{4,5},{5,4},{6,7},{7,6},{8,9},{9,8},{10,11... | collective-permute-start | bytes 589832 | tf_op jit(solution)/shard_map/ppermute | solution.py:235
  139.0 4.7 %collective-permute-start.37 = (bf16[256,384]{1,0:T(8,128)(2,1)S(1)}, bf16[256,384]{1,0:T(8,128)(2,1)}, u32[]{:S(2)}, u32[]{:S(2)}) collective-permute-start(bf16[256,384]{1,0:T(8,128)(2,1)S(1)} %collective-permute-done.28.refs_7_), channel_id=1, source_target_pairs={{0,1},{1,0},{2,3},{3,2},{4,5},{5,4},{6,7},{7,6},{8,9},{9,8},{10,11... | collective-permute-start | bytes 589832 | tf_op jit(solution)/shard_map/ppermute | solution.py:235
  139.5 14.8 %collective-permute-start.39 = (bf16[704,256]{1,0:T(8,128)(2,1)S(1)}, bf16[704,256]{1,0:T(8,128)(2,1)S(1)}, u32[]{:S(2)}, u32[]{:S(2)}) collective-permute-start(bf16[704,256]{1,0:T(8,128)(2,1)S(1)} %get-tuple-element.171.b_own), channel_id=1, source_target_pairs={{0,1},{1,0},{2,3},{3,2},{4,5},{5,4},{6,7},{7,6},{8,9},{9,8},{10,11... | collective-permute-start | bytes 1081352 | tf_op jit(solution)/shard_map/ppermute | solution.py:235
  140.1 22.8 %collective-permute-start.41 = (bf16[704,256]{1,0:T(8,128)(2,1)S(1)}, bf16[704,256]{1,0:T(8,128)(2,1)S(1)}, u32[]{:S(2)}, u32[]{:S(2)}) collective-permute-start(bf16[704,256]{1,0:T(8,128)(2,1)S(1)} %get-tuple-element.171.b_own), channel_id=1, source_target_pairs={{8,0},{12,8},{4,12},{0,4},{9,1},{13,9},{5,13},{1,5},{10,2},{14,10}... | collective-permute-start | bytes 1081352 | tf_op jit(solution)/shard_map/ppermute | solution.py:235
  141.0 13.3 %collective-permute-start.38 = (bf16[704,256]{1,0:T(8,128)(2,1)S(1)}, bf16[704,256]{1,0:T(8,128)(2,1)S(1)}, u32[]{:S(2)}, u32[]{:S(2)}) collective-permute-start(bf16[704,256]{1,0:T(8,128)(2,1)S(1)} %get-tuple-element.172.a_own), channel_id=1, source_target_pairs={{0,1},{1,0},{2,3},{3,2},{4,5},{5,4},{6,7},{7,6},{8,9},{9,8},{10,11... | collective-permute-start | bytes 1081352 | tf_op jit(solution)/shard_map/ppermute | solution.py:235
  141.2 21.3 %collective-permute-start.42 = (bf16[704,256]{1,0:T(8,128)(2,1)S(1)}, bf16[704,256]{1,0:T(8,128)(2,1)S(1)}, u32[]{:S(2)}, u32[]{:S(2)}) collective-permute-start(bf16[704,256]{1,0:T(8,128)(2,1)S(1)} %get-tuple-element.172.a_own), channel_id=1, source_target_pairs={{0,8},{8,12},{12,4},{4,0},{1,9},{9,13},{13,5},{5,1},{2,10},{10,14}... | collective-permute-start | bytes 1081352 | tf_op jit(solution)/shard_map/ppermute | solution.py:235
  162.5 3.1 %collective-permute-start.45 = (bf16[704,256]{1,0:T(8,128)(2,1)S(1)}, bf16[704,256]{1,0:T(8,128)(2,1)S(1)}, u32[]{:S(2)}, u32[]{:S(2)}) collective-permute-start(bf16[704,256]{1,0:T(8,128)(2,1)S(1)} %collective-permute-done.42.a_own), channel_id=1, source_target_pairs={{0,1},{1,0},{2,3},{3,2},{4,5},{5,4},{6,7},{7,6},{8,9},{9,8},{10,11... | collective-permute-start | bytes 1081352 | tf_op jit(solution)/shard_map/ppermute | solution.py:235
  162.8 4.0 %collective-permute-start.46 = (bf16[704,256]{1,0:T(8,128)(2,1)S(1)}, bf16[704,256]{1,0:T(8,128)(2,1)S(1)}, u32[]{:S(2)}, u32[]{:S(2)}) collective-permute-start(bf16[704,256]{1,0:T(8,128)(2,1)S(1)} %collective-permute-done.41.b_own), channel_id=1, source_target_pairs={{0,1},{1,0},{2,3},{3,2},{4,5},{5,4},{6,7},{7,6},{8,9},{9,8},{10,11... | collective-permute-start | bytes 1081352 | tf_op jit(solution)/shard_map/ppermute | solution.py:235
  163.1 11.1 %collective-permute-start.44 = (bf16[704,256]{1,0:T(8,128)(2,1)S(1)}, bf16[704,256]{1,0:T(8,128)(2,1)S(1)}, u32[]{:S(2)}, u32[]{:S(2)}) collective-permute-start(bf16[704,256]{1,0:T(8,128)(2,1)S(1)} %collective-permute-done.42.a_own), channel_id=1, source_target_pairs={{0,8},{8,12},{12,4},{4,0},{1,9},{9,13},{13,5},{5,1},{2,10},{10,14}... | collective-permute-start | bytes 1081352 | tf_op jit(solution)/shard_map/ppermute | solution.py:235
  164.1 18.4 %collective-permute-start.43 = (bf16[704,256]{1,0:T(8,128)(2,1)S(1)}, bf16[704,256]{1,0:T(8,128)(2,1)S(1)}, u32[]{:S(2)}, u32[]{:S(2)}) collective-permute-start(bf16[704,256]{1,0:T(8,128)(2,1)S(1)} %collective-permute-done.41.b_own), channel_id=1, source_target_pairs={{8,0},{12,8},{4,12},{0,4},{9,1},{13,9},{5,13},{1,5},{10,2},{14,10}... | collective-permute-start | bytes 1081352 | tf_op jit(solution)/shard_map/ppermute | solution.py:235
  165.1 18.0 %collective-permute-start.40 = (bf16[2,384,256]{2,1,0:T(8,128)(2,1)}, bf16[2,384,256]{2,1,0:T(8,128)(2,1)S(1)}, u32[]{:S(2)}, u32[]{:S(2)}) collective-permute-start(bf16[2,384,256]{2,1,0:T(8,128)(2,1)} %get-tuple-element.131), channel_id=1, source_target_pairs={{0,16},{16,0},{1,17},{17,1},{2,18},{18,2},{3,19},{19,3},{4,20},{20... | collective-permute-start | bytes 1179656 | tf_op jit(solution)/shard_map/ppermute | solution.py:235
  165.7 18.9 %collective-permute-start.47 = (bf16[2,384,256]{2,1,0:T(8,128)(2,1)}, bf16[2,384,256]{2,1,0:T(8,128)(2,1)S(1)}, u32[]{:S(2)}, u32[]{:S(2)}) collective-permute-start(bf16[2,384,256]{2,1,0:T(8,128)(2,1)} %get-tuple-element.140), channel_id=1, source_target_pairs={{0,2},{2,0},{1,3},{3,1},{4,6},{6,4},{5,7},{7,5},{8,10},{10,8},{9,1... | collective-permute-start | bytes 1179656 | tf_op jit(solution)/shard_map/ppermute | solution.py:235
  174.2 13.1 %collective-permute-start.53 = (bf16[704,256]{1,0:T(8,128)(2,1)S(1)}, bf16[704,256]{1,0:T(8,128)(2,1)S(1)}, u32[]{:S(2)}, u32[]{:S(2)}) collective-permute-start(bf16[704,256]{1,0:T(8,128)(2,1)S(1)} %collective-permute-done.44.a_own), channel_id=1, source_target_pairs={{0,1},{1,0},{2,3},{3,2},{4,5},{5,4},{6,7},{7,6},{8,9},{9,8},{10,11... | collective-permute-start | bytes 1081352 | tf_op jit(solution)/shard_map/ppermute | solution.py:235
  182.5 6.4 %collective-permute-start.54 = (bf16[704,256]{1,0:T(8,128)(2,1)S(1)}, bf16[704,256]{1,0:T(8,128)(2,1)}, u32[]{:S(2)}, u32[]{:S(2)}) collective-permute-start(bf16[704,256]{1,0:T(8,128)(2,1)S(1)} %collective-permute-done.43.b_own), channel_id=1, source_target_pairs={{0,1},{1,0},{2,3},{3,2},{4,5},{5,4},{6,7},{7,6},{8,9},{9,8},{10,11... | collective-permute-start | bytes 1081352 | tf_op jit(solution)/shard_map/ppermute | solution.py:235
  182.5 13.1 %collective-permute-start.52 = (bf16[704,256]{1,0:T(8,128)(2,1)S(1)}, bf16[704,256]{1,0:T(8,128)(2,1)S(1)}, u32[]{:S(2)}, u32[]{:S(2)}) collective-permute-start(bf16[704,256]{1,0:T(8,128)(2,1)S(1)} %collective-permute-done.44.a_own), channel_id=1, source_target_pairs={{0,8},{8,12},{12,4},{4,0},{1,9},{9,13},{13,5},{5,1},{2,10},{10,14}... | collective-permute-start | bytes 1081352 | tf_op jit(solution)/shard_map/ppermute | solution.py:235
  183.1 18.1 %collective-permute-start.51 = (bf16[704,256]{1,0:T(8,128)(2,1)S(1)}, bf16[704,256]{1,0:T(8,128)(2,1)S(1)}, u32[]{:S(2)}, u32[]{:S(2)}) collective-permute-start(bf16[704,256]{1,0:T(8,128)(2,1)S(1)} %collective-permute-done.43.b_own), channel_id=1, source_target_pairs={{8,0},{12,8},{4,12},{0,4},{9,1},{13,9},{5,13},{1,5},{10,2},{14,10}... | collective-permute-start | bytes 1081352 | tf_op jit(solution)/shard_map/ppermute | solution.py:235
  184.5 17.2 %collective-permute-start.50 = (bf16[2,384,256]{2,1,0:T(8,128)(2,1)}, bf16[2,384,256]{2,1,0:T(8,128)(2,1)S(1)}, u32[]{:S(2)}, u32[]{:S(2)}) collective-permute-start(bf16[2,384,256]{2,1,0:T(8,128)(2,1)} %get-tuple-element.144), channel_id=1, source_target_pairs={{0,16},{16,0},{1,17},{17,1},{2,18},{18,2},{3,19},{19,3},{4,20},{20... | collective-permute-start | bytes 1179656 | tf_op jit(solution)/shard_map/ppermute | solution.py:235
  188.1 14.4 %collective-permute-start.55 = (bf16[2,384,256]{2,1,0:T(8,128)(2,1)}, bf16[2,384,256]{2,1,0:T(8,128)(2,1)S(1)}, u32[]{:S(2)}, u32[]{:S(2)}) collective-permute-start(bf16[2,384,256]{2,1,0:T(8,128)(2,1)} %get-tuple-element.151), channel_id=1, source_target_pairs={{0,2},{2,0},{1,3},{3,1},{4,6},{6,4},{5,7},{7,5},{8,10},{10,8},{9,1... | collective-permute-start | bytes 1179656 | tf_op jit(solution)/shard_map/ppermute | solution.py:235
  195.7 9.7 %collective-permute-start.59 = (bf16[704,256]{1,0:T(8,128)(2,1)S(1)}, bf16[704,256]{1,0:T(8,128)(2,1)S(1)}, u32[]{:S(2)}, u32[]{:S(2)}) collective-permute-start(bf16[704,256]{1,0:T(8,128)(2,1)S(1)} %collective-permute-done.52.a_own), channel_id=1, source_target_pairs={{0,1},{1,0},{2,3},{3,2},{4,5},{5,4},{6,7},{7,6},{8,9},{9,8},{10,11... | collective-permute-start | bytes 1081352 | tf_op jit(solution)/shard_map/ppermute | solution.py:235
  201.2 4.2 %collective-permute-start.60 = (bf16[704,256]{1,0:T(8,128)(2,1)S(1)}, bf16[704,256]{1,0:T(8,128)(2,1)S(1)}, u32[]{:S(2)}, u32[]{:S(2)}) collective-permute-start(bf16[704,256]{1,0:T(8,128)(2,1)S(1)} %collective-permute-done.51.b_own), channel_id=1, source_target_pairs={{0,1},{1,0},{2,3},{3,2},{4,5},{5,4},{6,7},{7,6},{8,9},{9,8},{10,11... | collective-permute-start | bytes 1081352 | tf_op jit(solution)/shard_map/ppermute | solution.py:235
  201.2 15.8 %collective-permute-start.58 = (bf16[2,384,256]{2,1,0:T(8,128)(2,1)}, bf16[2,384,256]{2,1,0:T(8,128)(2,1)S(1)}, u32[]{:S(2)}, u32[]{:S(2)}) collective-permute-start(bf16[2,384,256]{2,1,0:T(8,128)(2,1)} %get-tuple-element.155), channel_id=1, source_target_pairs={{0,16},{16,0},{1,17},{17,1},{2,18},{18,2},{3,19},{19,3},{4,20},{20... | collective-permute-start | bytes 1179656 | tf_op jit(solution)/shard_map/ppermute | solution.py:235
  201.7 15.9 %collective-permute-start.61 = (bf16[2,384,256]{2,1,0:T(8,128)(2,1)}, bf16[2,384,256]{2,1,0:T(8,128)(2,1)S(1)}, u32[]{:S(2)}, u32[]{:S(2)}) collective-permute-start(bf16[2,384,256]{2,1,0:T(8,128)(2,1)} %get-tuple-element.160), channel_id=1, source_target_pairs={{0,2},{2,0},{1,3},{3,1},{4,6},{6,4},{5,7},{7,5},{8,10},{10,8},{9,1... | collective-permute-start | bytes 1179656 | tf_op jit(solution)/shard_map/ppermute | solution.py:235
  213.5 12.2 %collective-permute-start.64 = (bf16[2,384,256]{2,1,0:T(8,128)(2,1)}, bf16[2,384,256]{2,1,0:T(8,128)(2,1)S(1)}, u32[]{:S(2)}, u32[]{:S(2)}) collective-permute-start(bf16[2,384,256]{2,1,0:T(8,128)(2,1)} %get-tuple-element.164), channel_id=1, source_target_pairs={{0,16},{16,0},{1,17},{17,1},{2,18},{18,2},{3,19},{19,3},{4,20},{20... | collective-permute-start | bytes 1179656 | tf_op jit(solution)/shard_map/ppermute | solution.py:235
  215.0 12.2 %collective-permute-start.65 = (bf16[2,384,256]{2,1,0:T(8,128)(2,1)}, bf16[2,384,256]{2,1,0:T(8,128)(2,1)S(1)}, u32[]{:S(2)}, u32[]{:S(2)}) collective-permute-start(bf16[2,384,256]{2,1,0:T(8,128)(2,1)} %get-tuple-element.167), channel_id=1, source_target_pairs={{0,2},{2,0},{1,3},{3,1},{4,6},{6,4},{5,7},{7,5},{8,10},{10,8},{9,1... | collective-permute-start | bytes 1179656 | tf_op jit(solution)/shard_map/ppermute | solution.py:235
  216.2 15.2 %collective-permute-start.48 = (bf16[384,256]{1,0:T(8,128)(2,1)}, bf16[384,256]{1,0:T(8,128)(2,1)S(1)}, u32[]{:S(2)}, u32[]{:S(2)}) collective-permute-start(bf16[384,256]{1,0:T(8,128)(2,1)} %get-tuple-element.142), channel_id=1, source_target_pairs={{0,2},{2,0},{1,3},{3,1},{4,6},{6,4},{5,7},{7,5},{8,10},{10,8},{9,1... | collective-permute-start | bytes 589832 | tf_op jit(solution)/shard_map/ppermute | solution.py:235
  217.0 14.9 %collective-permute-start.49 = (bf16[384,256]{1,0:T(8,128)(2,1)S(1)}, bf16[384,256]{1,0:T(8,128)(2,1)S(1)}, u32[]{:S(2)}, u32[]{:S(2)}) collective-permute-start(bf16[384,256]{1,0:T(8,128)(2,1)S(1)} %copy-done.51), channel_id=1, source_target_pairs={{0,16},{16,0},{1,17},{17,1},{2,18},{18,2},{3,19},{19,3},{4,20},{20... | collective-permute-start | bytes 589832 | tf_op jit(solution)/shard_map/ppermute | solution.py:235
  217.6 18.0 %collective-permute-start.56 = (bf16[384,256]{1,0:T(8,128)(2,1)}, bf16[384,256]{1,0:T(8,128)(2,1)S(1)}, u32[]{:S(2)}, u32[]{:S(2)}) collective-permute-start(bf16[384,256]{1,0:T(8,128)(2,1)} %get-tuple-element.153), channel_id=1, source_target_pairs={{0,2},{2,0},{1,3},{3,1},{4,6},{6,4},{5,7},{7,5},{8,10},{10,8},{9,1... | collective-permute-start | bytes 589832 | tf_op jit(solution)/shard_map/ppermute | solution.py:235
  225.7 10.5 %collective-permute-start.57 = (bf16[384,256]{1,0:T(8,128)(2,1)}, bf16[384,256]{1,0:T(8,128)(2,1)S(1)}, u32[]{:S(2)}, u32[]{:S(2)}) collective-permute-start(bf16[384,256]{1,0:T(8,128)(2,1)} %get-tuple-element.154), channel_id=1, source_target_pairs={{0,16},{16,0},{1,17},{17,1},{2,18},{18,2},{3,19},{19,3},{4,20},{20... | collective-permute-start | bytes 589832 | tf_op jit(solution)/shard_map/ppermute | solution.py:235
  227.2 12.6 %collective-permute-start.62 = (bf16[384,256]{1,0:T(8,128)(2,1)}, bf16[384,256]{1,0:T(8,128)(2,1)S(1)}, u32[]{:S(2)}, u32[]{:S(2)}) collective-permute-start(bf16[384,256]{1,0:T(8,128)(2,1)} %get-tuple-element.162), channel_id=1, source_target_pairs={{0,2},{2,0},{1,3},{3,1},{4,6},{6,4},{5,7},{7,5},{8,10},{10,8},{9,1... | collective-permute-start | bytes 589832 | tf_op jit(solution)/shard_map/ppermute | solution.py:235
  231.4 8.4 %collective-permute-start.63 = (bf16[384,256]{1,0:T(8,128)(2,1)}, bf16[384,256]{1,0:T(8,128)(2,1)S(1)}, u32[]{:S(2)}, u32[]{:S(2)}) collective-permute-start(bf16[384,256]{1,0:T(8,128)(2,1)} %get-tuple-element.163), channel_id=1, source_target_pairs={{0,16},{16,0},{1,17},{17,1},{2,18},{18,2},{3,19},{19,3},{4,20},{20... | collective-permute-start | bytes 589832 | tf_op jit(solution)/shard_map/ppermute | solution.py:235
  231.9 10.8 %collective-permute-start.66 = (bf16[384,256]{1,0:T(8,128)(2,1)}, bf16[384,256]{1,0:T(8,128)(2,1)S(1)}, u32[]{:S(2)}, u32[]{:S(2)}) collective-permute-start(bf16[384,256]{1,0:T(8,128)(2,1)} %get-tuple-element.169), channel_id=1, source_target_pairs={{0,2},{2,0},{1,3},{3,1},{4,6},{6,4},{5,7},{7,5},{8,10},{10,8},{9,1... | collective-permute-start | bytes 589832 | tf_op jit(solution)/shard_map/ppermute | solution.py:235
  235.6 7.1 %collective-permute-start.67 = (bf16[384,256]{1,0:T(8,128)(2,1)}, bf16[384,256]{1,0:T(8,128)(2,1)S(1)}, u32[]{:S(2)}, u32[]{:S(2)}) collective-permute-start(bf16[384,256]{1,0:T(8,128)(2,1)} %get-tuple-element.170), channel_id=1, source_target_pairs={{0,16},{16,0},{1,17},{17,1},{2,18},{18,2},{3,19},{19,3},{4,20},{20... | collective-permute-start | bytes 589832 | tf_op jit(solution)/shard_map/ppermute | solution.py:235
  (63 other events, 671.6 us)

commit v2 on v1

v2 whole, which is shorter than its diff:
```python
import functools

import jax
import jax.numpy as jnp
from jax import lax
from jax.experimental import pallas as pl
from jax.experimental.pallas import tpu as pltpu
from jax.sharding import Mesh
from jax.sharding import PartitionSpec as P


BF16 = jnp.bfloat16
F32 = jnp.float32
LANES = 128
EPS = 1e-06


def general_plan(
    tokens, norm_gain, gate_weight, up_weight, gate_scale, up_scale, down_weight, down_scale
):
    values = tokens.astype(F32)
    own_normed = (
        values * lax.rsqrt(jnp.mean(values * values, axis=-1, keepdims=True) + EPS) * norm_gain
    ).astype(BF16)
    normed = lax.all_gather(own_normed, "tp", axis=0, tiled=True)
    gate_whole = lax.all_gather(gate_weight.astype(BF16), "fs", axis=0, tiled=True)
    up_whole = lax.all_gather(up_weight.astype(BF16), "fs", axis=0, tiled=True)
    gate_value = jnp.dot(normed, gate_whole, preferred_element_type=F32)
    up_value = jnp.dot(normed, up_whole, preferred_element_type=F32)
    hidden = (jax.nn.silu(gate_value * gate_scale) * (up_value * up_scale)).astype(BF16)
    down_whole = lax.all_gather(down_weight.astype(BF16), "fs", axis=1, tiled=True)
    partial_value = jnp.dot(hidden, down_whole, preferred_element_type=F32).astype(BF16)
    summed = lax.psum_scatter(partial_value, "tp", scatter_dimension=0, tiled=True).astype(F32)
    return (summed * down_scale).astype(BF16)


def pick(index, table):
    value = jnp.int32(table[0])
    for at, entry in enumerate(table[1:], 1):
        value = jnp.where(index == at, jnp.int32(entry), value)
    return value


def ring_order(count):
    return list(range(0, count, 2)) + list(range(1, count, 2))[::-1]


def ring_source(count, step):
    ring = ring_order(count)
    return [ring[(ring.index(z) - step) % count] for z in range(count)]


VM = pl.BlockSpec(memory_space=pltpu.VMEM)
ANY = pl.BlockSpec(memory_space=pltpu.HBM)


def call(kernel, outs, ins, *, flops=0, nbytes=0, **kw):
    kw.setdefault("in_specs", [VM] * len(ins))
    kw.setdefault("out_specs", [VM] * len(outs))
    return pl.pallas_call(
        kernel,
        out_shape=[jax.ShapeDtypeStruct(s, d) for s, d in outs],
        cost_estimate=pl.CostEstimate(
            flops=int(flops), bytes_accessed=int(nbytes), transcendentals=0
        ),
        **kw,
    )(*ins)


def norm_kernel(lo, t_ref, g_ref, lo_ref, hi_ref):
    rows = t_ref.shape[0]
    for at in range(0, rows, lo):
        v = t_ref[at : at + lo, :].astype(F32)
        v = v * lax.rsqrt(jnp.mean(v * v, axis=-1, keepdims=True) + EPS) * g_ref[...]
        if at == 0:
            lo_ref[...] = v.astype(BF16)
        else:
            hi_ref[at - lo : at, :] = v.astype(BF16)


def prep_kernel(full, first, which, g_ref, u_ref, *refs):
    outs, (held, sems) = refs[:-2], refs[-2:]
    x, y = lax.axis_index("x"), lax.axis_index("y")
    half = LANES // 2
    second = full - first
    copies, at = [], 0

    def fetch(src, start, n):
        nonlocal at
        dst = held.at[:, pl.ds(at, n)]
        copy = pltpu.make_async_copy(src.at[:, pl.ds(start, n)], dst, sems.at[len(copies)])
        copy.start()
        copies.append((copy, at, n))
        at += n

    for far, late in which:
        q = 2 * x + (1 - y if far else y)
        start = pl.multiple_of(q * full + (first if late else 0), LANES)
        for src in (g_ref, u_ref):
            fetch(src, start, second if late else first)
        if late:
            start = pl.multiple_of(4 * full + (q // 2) * LANES, LANES)
            for src in (g_ref, u_ref):
                fetch(src, start, LANES)
    rest = list(copies)

    def arrived():
        copy, at, n = rest.pop(0)
        copy.wait()
        return held[:, at : at + n]

    for out, (far, late) in zip(outs, which):
        odd = ((1 - y if far else y) % 2) == 1
        n = second if late else first
        out[:, :n] = arrived().astype(BF16)
        out[:, n : 2 * n] = arrived().astype(BF16)
        if late:
            g, u = arrived(), arrived()
            g = jnp.where(odd, pltpu.roll(g, half, 1), g)
            u = jnp.where(odd, u, pltpu.roll(u, half, 1))
            lane = lax.broadcasted_iota(jnp.int32, g.shape, 1)
            out[:, 2 * n :] = jnp.where(lane < half, g, u).astype(BF16)


def scale_kernel(full, first, g_ref, u_ref, out):
    x, y = lax.axis_index("x"), lax.axis_index("y")
    q, half = 2 * x + y, LANES // 2
    at = 0
    for lo, hi in ((0, first), (first, full)):
        for ref in (g_ref, u_ref):
            for k in range(lo // LANES, hi // LANES):
                out[:, at : at + LANES] = ref[pl.ds(q * (full // LANES) + k, 1), :]
                at += LANES
    row = pl.ds(4 * full // LANES + q // 2, 1)
    odd = (q % 2) == 1
    g, u = g_ref[row, :], u_ref[row, :]
    g = jnp.where(odd, pltpu.roll(g, half, 1), g)
    u = jnp.where(odd, u, pltpu.roll(u, half, 1))
    out[:, at:] = jnp.where(lax.broadcasted_iota(jnp.int32, g.shape, 1) < half, g, u)


def down_prep_kernel(full, d_ref, own, other):
    x, y = lax.axis_index("x"), lax.axis_index("y")
    half = LANES // 2
    for q, out in ((2 * x + y, own), (2 * x + 1 - y, other)):
        out[:full, :] = d_ref[pl.ds(pl.multiple_of(q * full, 64), full), :].astype(BF16)
        out[full:, :] = d_ref[pl.ds(pl.multiple_of(4 * full + q * half, 64), half), :].astype(BF16)


def gate_up_kernel(nz, blk, part, cols, slots, s_own, s_oth, *refs):
    tokens, refs = refs[: 2 * slots], refs[2 * slots :]
    pieces, (out, xs, w, xsem, wsem) = refs[: 4 * nz], refs[4 * nz :]
    y, z = lax.axis_index("y"), lax.axis_index("z")
    n = pieces[0].shape[1]
    lo = tokens[0].shape[0]
    i = pl.program_id(0)

    @pl.when(i == 0)
    def _():
        copies = []
        for s in range(nz):
            f = 2 * pick(z, ring_source(nz, s)) + y
            b = 2 * pick(z, ring_source(nz, -s)) + 1 - y
            for k, at in enumerate((f, b, f, b)):
                rows = pl.ds(pl.multiple_of(at * blk, blk), blk)
                dst = w.at[rows, pl.ds(n * (k // 2), n)]
                copies.append(pltpu.make_async_copy(pieces[k * nz + s], dst, wsem.at[4 * s + k]))
        for c in copies:
            c.start()
        for k, ref in enumerate(tokens):
            rows = pl.ds(lo, ref.shape[0]) if k % 2 else pl.ds(0, lo)
            pltpu.make_async_copy(ref, xs.at[k // 2, rows], xsem.at[k]).start()
        for c in copies:
            c.wait()

    pltpu.make_async_copy(tokens[0], xs.at[i, pl.ds(0, lo)], xsem.at[2 * i]).wait()
    rest = xs.shape[1] - lo
    pltpu.make_async_copy(tokens[1], xs.at[i, pl.ds(lo, rest)], xsem.at[2 * i + 1]).wait()
    value = jnp.dot(xs[i], w[...], preferred_element_type=F32)
    tails = []
    for at, scale in ((0, s_own), (1, s_oth)):
        v = value[:, at * n : (at + 1) * n] * scale[:, cols : cols + n]
        g, u = v[:, :part], v[:, part : 2 * part]
        out[:, at * part : (at + 1) * part] = (g / (1 + jnp.exp(-g)) * u).astype(BF16)
        if n > 2 * part:
            m = v[:, 2 * part :]
            tails.append(m / (1 + jnp.exp(-m)) * pltpu.roll(m, LANES // 2, 1))
    if tails:
        h, o = tails
        lane = lax.broadcasted_iota(jnp.int32, h.shape, 1)
        o = pltpu.roll(o, LANES // 2, 1)
        out[:, 2 * part :] = jnp.where(lane < LANES // 2, h, o).astype(BF16)


def down_kernel(cuts, count, h1, h2, *refs):
    pieces, refs = refs[: 4 * count], refs[4 * count :]
    ax_keep, ax_send, ay_keep, ay_send, w, sems = refs
    i = pl.program_id(0)
    blk = pieces[0].shape[1]
    rows = h1.shape[0] // 2

    @pl.when(i == 0)
    def _():
        copies = []
        for k in range(2 * count):
            cols = pl.ds(((k % 2) * count + k // 2) * blk, blk)
            at = 0
            for lo, hi in cuts:
                for piece in pieces[2 * k : 2 * k + 2]:
                    src, dst = piece.at[pl.ds(lo, hi - lo), :], w.at[pl.ds(at, hi - lo), cols]
                    copies.append(pltpu.make_async_copy(src, dst, sems.at[len(copies)]))
                    at += hi - lo
        for copy in copies:
            copy.start()
        for copy in copies:
            copy.wait()

    n = h1.shape[1]
    value = jnp.dot(h1[...], w[:n], preferred_element_type=F32) + jnp.dot(
        h2[...], w[n:], preferred_element_type=F32
    )
    value = value.astype(BF16)
    left, right = value[:, : count * blk], value[:, count * blk :]
    ay_keep[0], ay_send[0] = right[:rows], right[rows:]

    @pl.when(i == 0)
    def _():
        ax_keep[0], ax_keep[1] = left[:rows], left[rows:]

    @pl.when(i == 1)
    def _():
        ax_send[0], ax_send[1] = left[:rows], left[rows:]


def second_add_kernel(ax_keep, ax_got, ay_keep, ay_got, ax, ay):
    ax[...] = (ax_keep[0].astype(F32) + ax_got[0].astype(F32)).astype(BF16)
    ay[...] = (ay_keep[0].astype(F32) + ay_got[0].astype(F32)).astype(BF16)


def final_kernel(nz, blk, groups, aliased, *refs):
    ins, scale, refs = refs[: 6 * len(groups)], refs[6 * len(groups)], refs[6 * len(groups) + 1 :]
    out, held, sems = refs[1:] if aliased else refs
    z = lax.axis_index("z")
    copies = []
    for n, group in enumerate(groups):
        for j in range(2):
            a, b, c = ins[6 * n + 3 * j : 6 * n + 3 * j + 3]
            for k, s in enumerate(group):
                source = pick(z, ring_source(nz, s if j == 0 else -s))
                at = pl.ds(pl.multiple_of((2 * source + j) * blk, blk), blk)
                here = slice(k * blk, (k + 1) * blk)
                value = a[0, :, here].astype(F32) + b[0, :, here].astype(F32)
                value = value + c[:, here].astype(F32)
                slot = len(copies)
                held[slot] = (value * scale[:, at]).astype(BF16)
                copies.append(pltpu.make_async_copy(held.at[slot], out.at[:, at], sems.at[slot]))
                copies[-1].start()
    for copy in copies:
        copy.wait()


def after(value, *others):
    return lax.optimization_barrier((value, *others))[0]


def pair_plan(
    nz, tokens, norm_gain, gate_weight, up_weight, gate_scale, up_scale, down_weight, down_scale
):
    rows, width = tokens.shape
    blk, ffl = gate_weight.shape
    full = ffl // (4 * LANES) * LANES
    quarter = ffl // 4
    first = -(-full // (2 * LANES)) * LANES
    second = full - first
    wide1, wide2 = 2 * first, 2 * second + LANES
    lo = rows // 3
    ring = ring_order(nz)
    ahead = [(ring[p], ring[(p + 1) % nz]) for p in range(nz)]
    back = [(b, a) for a, b in ahead]
    swap = [(0, 1), (1, 0)]
    y = lax.axis_index("y")

    def send(v, axis, hops=swap):
        return lax.ppermute(v, axis, hops)

    def prep(which, *ins):
        wides = [wide2 if late else wide1 for _, late in which]
        held = sum(w + (LANES if late else 0) for w, (_, late) in zip(wides, which))
        return call(
            functools.partial(prep_kernel, full, first, which),
            [((blk, w), BF16) for w in wides],
            list(ins),
            in_specs=[ANY, ANY],
            scratch_shapes=[
                pltpu.VMEM((blk, held), F32),
                pltpu.SemaphoreType.DMA((4 * len(which),)),
            ],
            flops=blk * sum(wides),
            nbytes=blk * sum(wides) * 6,
        )

    (own1,) = prep(((False, False),), gate_weight, up_weight)
    far1, own2, far2 = prep(
        ((True, False), (False, True), (True, True)), after(gate_weight, own1), up_weight
    )
    hop = lambda v: send(v, "z", ahead)
    pop = lambda v: send(v, "z", back)
    c1, c2 = [own1, hop(own1)], [own2, hop(own2)]
    g1, g2 = [send(far1, "y")], [send(far2, "y")]
    n_lo, n_hi = call(
        functools.partial(norm_kernel, lo),
        [((lo, width), BF16), ((rows - lo, width), BF16)],
        [after(tokens, own2), norm_gain.reshape(1, -1)],
        flops=rows * width * 8,
        nbytes=rows * width * 4,
    )
    hi_x, hi_y = send(n_hi, "x"), send(n_hi, "y")
    d_own, d_nbr = call(
        functools.partial(down_prep_kernel, full),
        [((quarter, blk), BF16), ((quarter, blk), BF16)],
        [after(down_weight, n_hi)],
        flops=blk * ffl,
        nbytes=blk * ffl * 6,
    )
    (scale,) = call(
        functools.partial(scale_kernel, full, first),
        [((1, 2 * quarter), F32)],
        [after(v, d_own).reshape(-1, LANES) for v in (gate_scale, up_scale)],
        flops=ffl,
        nbytes=ffl * 8,
    )
    scale_oth = send(scale, "c")
    clock = scale

    def event(value):
        nonlocal clock
        clock = after(value, clock)
        return clock

    across = {}

    def twin(name, v):
        across[name] = send(v, "c")

    twin("c10", own1)
    twin("c20", own2)
    c1[1] = event(c1[1])
    c1.append(hop(c1[1]))
    twin("c11", c1[1])
    lo_x = send(after(n_lo, clock), "x")
    g1[0] = event(g1[0])
    g1.append(pop(g1[0]))
    twin("g10", g1[0])
    c2[1] = event(c2[1])
    twin("c21", c2[1])
    g2[0] = event(g2[0])
    g2.append(pop(g2[0]))
    twin("g20", g2[0])
    lo_y = send(after(n_lo, clock), "y")
    c1[2] = event(c1[2])
    c1.append(hop(c1[2]))
    twin("c12", c1[2])
    g1[1] = event(g1[1])
    g1.append(pop(g1[1]))
    twin("g11", g1[1])
    c2.append(hop(after(c2[1], clock)))
    g2[1] = event(g2[1])
    g2.append(pop(g2[1]))
    twin("g21", g2[1])
    lo_x = event(lo_x)
    lo_xy = send(lo_x, "y")
    hi_y = event(hi_y)
    hi_xy = send(hi_y, "x")
    d_far = send(after(d_nbr, clock), "y")
    c1[3] = event(c1[3])
    twin("c13", c1[3])
    g1[2] = event(g1[2])
    g1.append(pop(g1[2]))
    twin("g12", g1[2])
    c2[2] = event(c2[2])
    c2.append(hop(c2[2]))
    twin("c22", c2[2])
    g2[2] = event(g2[2])
    g2.append(pop(g2[2]))
    twin("g22", g2[2])
    d_far = event(d_far)
    even = [jnp.where(y == 0, d_own, d_far)]
    odd = [jnp.where(y == 0, d_far, d_own)]
    even.append(hop(even[0]))
    odd.append(pop(odd[0]))
    twin("e0", even[0])
    twin("o0", odd[0])
    g1[3] = event(g1[3])
    twin("g13", g1[3])
    slots = [(n_lo, n_hi), (lo_y, hi_y), (lo_x, hi_x), (lo_xy, hi_xy)]

    def gate_up(at, own, far, part, slots):
        n = wide1 if at == 1 else wide2
        wide = 2 * part + (LANES if at == 2 else 0)
        twins = [across[f"c{at}{s}"] for s in range(nz)] + [across[f"g{at}{s}"] for s in range(nz)]
        count = len(slots)
        parts = [v for slot in slots for v in slot]
        parts[0] = after(parts[0], clock)
        return call(
            functools.partial(gate_up_kernel, nz, blk, part, 0 if at == 1 else wide1, count),
            [((count * rows, wide), BF16)],
            [scale, scale_oth, *parts, *own, *far, *twins],
            in_specs=[VM, VM] + [ANY] * (2 * count + 4 * nz),
            out_specs=[pl.BlockSpec((rows, wide), lambda i: (i, 0))],
            grid=(count,),
            scratch_shapes=[
                pltpu.VMEM((count, rows, width), BF16),
                pltpu.VMEM((width, 2 * n), BF16),
                pltpu.SemaphoreType.DMA((2 * count,)),
                pltpu.SemaphoreType.DMA((4 * nz,)),
            ],
            flops=count * rows * width * n * 4,
            nbytes=count * rows * (width + wide) * 2 + width * n * 4,
        )[0]

    h1 = gate_up(1, c1, g1, first, slots)
    clock = h1
    c2[3] = event(c2[3])
    twin("c23", c2[3])
    g2[3] = event(g2[3])
    twin("g23", g2[3])
    h2 = gate_up(2, c2, g2, second, slots)
    clock = h2

    def arrive(s):
        even[s], odd[s] = event(even[s]), event(odd[s])
        if s + 1 < nz:
            even.append(hop(even[s]))
            odd.append(pop(odd[s]))
        twin(f"e{s}", even[s])
        twin(f"o{s}", odd[s])

    arrive(1)

    cuts = ((0, first), (first, full), (full, quarter))

    def down(group):
        count = len(group)
        tile = lambda n: pl.BlockSpec((2 * rows, n), lambda i: (i, 0))
        both = pl.BlockSpec((2, rows, count * blk), lambda i: (0, 0, 0))
        slot = pl.BlockSpec((1, rows, count * blk), lambda i: (i, 0, 0))
        pieces = []
        for s in group:
            pieces += [even[s], across[f"e{s}"], odd[s], across[f"o{s}"]]
        return call(
            functools.partial(down_kernel, cuts, count),
            [((2, rows, count * blk), BF16)] * 4,
            [after(h1, clock), h2, *pieces],
            in_specs=[tile(h1.shape[1]), tile(h2.shape[1])] + [ANY] * (4 * count),
            out_specs=[both, both, slot, slot],
            grid=(2,),
            scratch_shapes=[
                pltpu.VMEM((2 * quarter, 2 * count * blk), BF16),
                pltpu.SemaphoreType.DMA((4 * count * len(cuts),)),
            ],
            flops=4 * rows * quarter * 8 * blk * count,
            nbytes=4 * rows * (2 * quarter + 2 * count * blk) * 2,
        )

    def second_add(count, *ins):
        one = pl.BlockSpec((1, rows, count * blk), lambda i: (1, 0, 0))
        whole = pl.BlockSpec((rows, count * blk), lambda i: (0, 0))
        return call(
            second_add_kernel,
            [((rows, count * blk), BF16)] * 2,
            list(ins),
            grid=(1,),
            in_specs=[one] * 4,
            out_specs=[whole] * 2,
            flops=4 * rows * blk * count,
            nbytes=2 * rows * blk * 6 * count,
        )

    groups = [list(range(nz))[:2]] + [[s] for s in range(2, nz)]
    parts = []
    flying = None

    def land():
        nonlocal clock
        _, count, ax_keep, ax_got, ay_keep, ay_got = flying
        ax_got, ay_got = event(ax_got), event(ay_got)
        ax_next, ay_next = second_add(count, ax_keep, ax_got, ay_keep, ay_got)
        clock = ax_next
        parts.extend([ax_keep, ax_got, send(ax_next, "y")])
        parts.extend([ay_keep, ay_got, send(ay_next, "x")])

    for n, group in enumerate(groups):
        ax_keep, ax_send, ay_keep, ay_send = down(group)
        clock = ax_keep
        ax_got, ay_got = send(ax_send, "x"), send(ay_send, "y")
        now = (n, len(group), ax_keep, ax_got, ay_keep, ay_got)
        if flying:
            land()
        if n + 1 < len(groups):
            for s in groups[n + 1]:
                if s > 1:
                    arrive(s)
        flying = now
    land()

    def final(some, made, done):
        specs = []
        for group in some:
            third = pl.BlockSpec((1, rows, len(group) * blk), lambda i: (0, 0, 0))
            flat = pl.BlockSpec((rows, len(group) * blk), lambda i: (0, 0))
            specs += [third, third, flat] * 2
        count = 2 * sum(map(len, some))
        aliased = [] if done is None else [done]
        return call(
            functools.partial(final_kernel, nz, blk, some, bool(aliased)),
            [((rows, width), BF16)],
            [*made, down_scale.reshape(1, -1), *aliased],
            grid=(1,),
            in_specs=specs + [VM] + [ANY] * len(aliased),
            out_specs=[ANY],
            scratch_shapes=[
                pltpu.VMEM((count, rows, blk), BF16),
                pltpu.SemaphoreType.DMA((count,)),
            ],
            input_output_aliases={6 * len(some) + 1: 0} if aliased else {},
            flops=rows * count * blk * 4,
            nbytes=rows * count * blk * 8,
        )[0]

    cut = len(groups) - 1
    made = parts[: 6 * cut]
    made[0] = after(made[0], clock)
    done = final(groups[:cut], made, None)
    return final(groups[cut:], parts[6 * cut :], done)


def solution(mesh):
    reps, shards, cores = (mesh.shape[a] for a in ("rep", "fs", "tp"))

    def run(*args):
        tokens, gate = args[0], args[2]
        rows = tokens.shape[0] // (reps * shards * cores)
        ffl, blk = gate.shape[1] // cores, gate.shape[0] // shards
        paired = (
            reps == 2
            and cores == 2
            and shards % 2 == 0
            and shards > 2
            and ffl % LANES == 0
            and ffl % (4 * LANES) == 2 * LANES
            and blk % LANES == 0
            and rows % 48 == 0
        )
        if paired:
            nz = shards // 2
            grid = Mesh(mesh.devices.reshape(reps, nz, 2, cores), ("x", "z", "y", "c"))
            row, deep, wide = ("x", "z", "y", "c"), ("z", "y"), "c"
            plan = functools.partial(pair_plan, nz)

            def body(*args):
                return plan(*args)

        else:
            grid, body = mesh, general_plan
            row, deep, wide = ("rep", "fs", "tp"), "fs", "tp"
        step = jax.shard_map(
            body,
            mesh=grid,
            in_specs=(
                P(row, None),
                P(),
                P(deep, wide),
                P(deep, wide),
                P(wide),
                P(wide),
                P(wide, deep),
                P(),
            ),
            out_specs=P(row, None),
            check_vma=False,
        )
        return step(*args)

    return run
```

time: 249 us -> 234 us (0.940)
  local copies, waits for them, and re-layouts: 23.4 us -> 10.6 us
  starting transfers between devices: 53.4 us -> 46.7 us
  waiting for transfers between devices: 89.8 us -> 95.1 us
    unnamed x125 -> x114, local copies, waits for them, and re-layouts: 18.7 us -> 10.6 us
    ppermute x68 -> x64, starting transfers between devices: 53.4 us -> 46.7 us  [send(): return lax.ppermute(v, axis, hops)]
    ppermute x68 -> x64, waiting for transfers between devices: 89.8 us -> 95.1 us  [send(): return lax.ppermute(v, axis, hops)]
  transfers between devices with their start and end apart: 68 -> 64, of which waited for: 19 -> 22; matrix products, arithmetic and copies ran while one was open for 6% -> 0% of each run, Pallas kernels for 29% -> 33%
where the time goes in v2:
time: 234 us; the launch traced here: 233 us
  waiting for transfers between devices  95.1 us (41%)
  Pallas kernels  80 us (34%)
  starting transfers between devices  46.7 us (20%)
  local copies, waits for them, and re-layouts  10.6 us (5%)
    ppermute x64, waiting for transfers between devices, send(): return lax.ppermute(v, axis, hops)  95.1 us
    pallas_call x15, Pallas kernels, call(): pl.pallas_call(kernel, out_shape=[jax.ShapeDtypeStruct(s, d) for s, d in...  80 us
    ppermute x64, starting transfers between devices, send(): return lax.ppermute(v, axis, hops)  46.7 us
    unnamed x114, local copies, waits for them, and re-layouts  10.6 us
  transfers between devices with their start and end apart: 64, of which 22 were waited for; matrix products, arithmetic and copies ran while one was open for 0% of the time, Pallas kernels for 33%

profile of v2, /device:TPU:0, one launch (start us, length us, event | category | flops | bytes accessed | tf_op | source)
XLA Modules:
  0.0 233.1 jit_solution(5026042422719599410)
XLA Ops:
  0.0 1.9 shard_map.82.refs_8_
  2.0 4.1 %collective-permute-start.2 = (bf16[256,768]{1,0:T(8,128)(2,1)}, bf16[256,768]{1,0:T(8,128)(2,1)S(1)}, u32[]{:S(2)}, u32[]{:S(2)}) collective-permute-start(bf16[256,768]{1,0:T(8,128)(2,1)} %shard_map.82.refs_8_), channel_id=1, source_target_pairs={{0,8},{8,12},{12,4},{4,0},{1,9},{9,13},{13,5},{5,1},{2,10},{10,14}... | collective-permute-start | bytes 1179656 | tf_op jit(solution)/shard_map/ppermute | solution.py:284
  6.1 2.7 %shard_map.83 = (bf16[256,768]{1,0:T(8,128)(2,1)}, bf16[256,640]{1,0:T(8,128)(2,1)}, bf16[256,640]{1,0:T(8,128)(2,1)}) custom-call(f32[256,2816]{1,0:T(8,128)} %g_ref.2, f32[256,2816]{1,0:T(8,128)} %u_ref.3), custom_call_target="tpu_custom_call" | custom-call | flops 524288 | bytes 3145728 | tf_op jit(solution)/shard_map/pallas_call | solution.py:60
  8.8 1.6 collective-permute-start.1
  10.3 1.6 collective-permute-start.6
  12.5 3.0 %shard_map.84 = (bf16[128,2048]{1,0:T(8,128)(2,1)}, bf16[256,2048]{1,0:T(8,128)(2,1)}) custom-call(bf16[384,2048]{1,0:T(8,128)(2,1)} %t_ref, f32[1,2048]{1,0:T(1,128)} %bitcast.8), custom_call_target="tpu_custom_call" | custom-call | flops 6291456 | bytes 3145728 | tf_op jit(solution)/shard_map/pallas_call | solution.py:60
  15.9 0.8 copy-done.24
  16.6 1.5 collective-permute-start.9
  18.2 2.7 %shard_map.85 = (bf16[704,256]{1,0:T(8,128)(2,1)}, bf16[704,256]{1,0:T(8,128)(2,1)}) custom-call(f32[2816,256]{1,0:T(8,128)} %d_ref), custom_call_target="tpu_custom_call" | custom-call | flops 720896 | bytes 4325376 | tf_op jit(solution)/shard_map/pallas_call | solution.py:60
  20.9 1.4 shard_map.86.s_own
  22.3 5.8 %collective-permute-done.5.refs_12_ = bf16[256,640]{1,0:T(8,128)(2,1)S(1)} collective-permute-done((bf16[256,640]{1,0:T(8,128)(2,1)}, bf16[256,640]{1,0:T(8,128)(2,1)S(1)}, u32[]{:S(2)}, u32[]{:S(2)}) %collective-permute-start.5) | collective-permute-done | bytes 327712 | tf_op jit(solution)/shard_map/ppermute | solution.py:284
  28.1 2.9 %collective-permute-start.4 = (bf16[256,768]{1,0:T(8,128)(2,1)}, bf16[256,768]{1,0:T(8,128)(2,1)S(1)}, u32[]{:S(2)}, u32[]{:S(2)}) collective-permute-start(bf16[256,768]{1,0:T(8,128)(2,1)} %copy-done.24), channel_id=1, source_target_pairs={{0,8},{8,12},{12,4},{4,0},{1,9},{9,13},{13,5},{5,1},{2,10},{10,14}... | collective-permute-start | bytes 1179656 | tf_op jit(solution)/shard_map/ppermute | solution.py:284
  31.0 1.4 collective-permute-done.s_oth
  32.4 1.5 collective-permute-start.10
  33.9 10.2 %collective-permute-done.11.refs_13_ = bf16[256,640]{1,0:T(8,128)(2,1)S(1)} collective-permute-done((bf16[256,640]{1,0:T(8,128)(2,1)S(1)}, bf16[256,640]{1,0:T(8,128)(2,1)S(1)}, u32[]{:S(2)}, u32[]{:S(2)}) %collective-permute-start.11) | collective-permute-done | bytes 327712 | tf_op jit(solution)/shard_map/ppermute | solution.py:284
  44.2 2.3 %collective-permute-done.4.refs_10_ = bf16[256,768]{1,0:T(8,128)(2,1)S(1)} collective-permute-done((bf16[256,768]{1,0:T(8,128)(2,1)}, bf16[256,768]{1,0:T(8,128)(2,1)S(1)}, u32[]{:S(2)}, u32[]{:S(2)}) %collective-permute-start.4) | collective-permute-done | bytes 393248 | tf_op jit(solution)/shard_map/ppermute | solution.py:284
  46.5 6.3 %collective-permute-done.3.refs_13_ = bf16[256,768]{1,0:T(8,128)(2,1)S(1)} collective-permute-done((bf16[256,768]{1,0:T(8,128)(2,1)}, bf16[256,768]{1,0:T(8,128)(2,1)S(1)}, u32[]{:S(2)}, u32[]{:S(2)}) %collective-permute-start.3) | collective-permute-done | bytes 393248 | tf_op jit(solution)/shard_map/ppermute | solution.py:284
  52.8 1.5 collective-permute-start.16
  54.9 1.5 collective-permute-start.17
  56.4 1.5 collective-permute-start.7
  57.9 1.5 collective-permute-start.15
  59.3 5.7 %collective-permute-done.16.refs_2_ = bf16[128,2048]{1,0:T(8,128)(2,1)S(1)} collective-permute-done((bf16[128,2048]{1,0:T(8,128)(2,1)S(1)}, bf16[128,2048]{1,0:T(8,128)(2,1)S(1)}, u32[]{:S(2)}, u32[]{:S(2)}) %collective-permute-start.16) | collective-permute-done | bytes 524320 | tf_op jit(solution)/shard_map/ppermute | solution.py:284
  65.1 1.5 collective-permute-start.13
  66.6 8.2 %collective-permute-done.8.refs_11_ = bf16[256,768]{1,0:T(8,128)(2,1)S(1)} collective-permute-done((bf16[256,768]{1,0:T(8,128)(2,1)S(1)}, bf16[256,768]{1,0:T(8,128)(2,1)S(1)}, u32[]{:S(2)}, u32[]{:S(2)}) %collective-permute-start.8) | collective-permute-done | bytes 393248 | tf_op jit(solution)/shard_map/ppermute | solution.py:284
  74.8 1.5 collective-permute-done.7.refs_14_
  76.4 13.9 %collective-permute-done.15.refs_10_ = bf16[256,640]{1,0:T(8,128)(2,1)} collective-permute-done((bf16[256,640]{1,0:T(8,128)(2,1)}, bf16[256,640]{1,0:T(8,128)(2,1)}, u32[]{:S(2)}, u32[]{:S(2)}) %collective-permute-start.15) | collective-permute-done | bytes 327712 | tf_op jit(solution)/shard_map/ppermute | solution.py:284
  90.9 8.1 %collective-permute-done.12.refs_15_ = bf16[256,768]{1,0:T(8,128)(2,1)S(1)} collective-permute-done((bf16[256,768]{1,0:T(8,128)(2,1)S(1)}, bf16[256,768]{1,0:T(8,128)(2,1)S(1)}, u32[]{:S(2)}, u32[]{:S(2)}) %collective-permute-start.12) | collective-permute-done | bytes 393248 | tf_op jit(solution)/shard_map/ppermute | solution.py:284
  100.1 8.0 %collective-permute-done.18.refs_6_ = bf16[128,2048]{1,0:T(8,128)(2,1)S(1)} collective-permute-done((bf16[128,2048]{1,0:T(8,128)(2,1)S(1)}, bf16[128,2048]{1,0:T(8,128)(2,1)S(1)}, u32[]{:S(2)}, u32[]{:S(2)}) %collective-permute-start.18) | collective-permute-done | bytes 524320 | tf_op jit(solution)/shard_map/ppermute | solution.py:284
  109.6 1.1 copy-done.19
  110.6 1.3 collective-permute-start.30
  112.0 16.6 %shard_map.87.h1 = bf16[1536,768]{1,0:T(8,128)(2,1)} custom-call(f32[1,1408]{1,0:T(1,128)} %shard_map.86.s_own, f32[1,1408]{1,0:T(1,128)} %copy-done.56, bf16[128,2048]{1,0:T(8,128)(2,1)} %get-tuple-element.108.refs_0_, bf16[256,2048]{1,0:T(8,128)(2,1)} %get-tuple-element.77.refs_1_, bf16[128,2048]{1,0:T(8,128)(2,1)} %copy-done.22, ...), custom_call_target="tpu_custom_call" | custom-call | flops 9663676416 | bytes 14942208 | tf_op jit(solution)/shard_map/pallas_call | solution.py:60
  130.5 1.6 collective-permute-start.29
  133.0 15.2 %shard_map.88.h2 = bf16[1536,640]{1,0:T(8,128)(2,1)} custom-call(f32[1,1408]{1,0:T(1,128)} %shard_map.86.s_own, f32[1,1408]{1,0:T(1,128)} %copy-done.56, bf16[128,2048]{1,0:T(8,128)(2,1)} %get-tuple-element.108.refs_0_, bf16[256,2048]{1,0:T(8,128)(2,1)} %get-tuple-element.77.refs_1_, bf16[128,2048]{1,0:T(8,128)(2,1)} %copy-done.22, ...), custom_call_target="tpu_custom_call" | custom-call | flops 8053063680 | bytes 13500416 | tf_op jit(solution)/shard_map/pallas_call | solution.py:60
  148.3 0.8 collective-permute-done.28.refs_6_
  149.6 1.6 collective-permute-start.41
  152.5 10.5 %shard_map.89 = (bf16[2,384,512]{2,1,0:T(8,128)(2,1)}, bf16[2,384,512]{2,1,0:T(8,128)(2,1)}, bf16[2,384,512]{2,1,0:T(8,128)(2,1)}, bf16[2,384,512]{2,1,0:T(8,128)(2,1)}) custom-call(bf16[1536,768]{1,0:T(8,128)(2,1)} %shard_map.87.h1, bf16[1536,640]{1,0:T(8,128)(2,1)} %shard_map.88.h2, bf16[704,256]{1,0:T(8,128)(2,1)} %copy-done.10, ...), custom_call_target="tpu_custom_call" | custom-call | flops 4429185024 | bytes 7471104 | tf_op jit(solution)/shard_map/pallas_call | solution.py:60
  163.1 1.5 collective-permute-start.48
  165.1 4.1 %collective-permute-done.40.refs_2_ = bf16[704,256]{1,0:T(8,128)(2,1)S(1)} collective-permute-done((bf16[704,256]{1,0:T(8,128)(2,1)S(1)}, bf16[704,256]{1,0:T(8,128)(2,1)S(1)}, u32[]{:S(2)}, u32[]{:S(2)}) %collective-permute-start.40) | collective-permute-done | bytes 360480 | tf_op jit(solution)/shard_map/ppermute | solution.py:284
  171.0 0.9 collective-permute-start.46
  171.8 0.8 copy-done.50
  172.6 7.1 %shard_map.90 = (bf16[2,384,256]{2,1,0:T(8,128)(2,1)}, bf16[2,384,256]{2,1,0:T(8,128)(2,1)}, bf16[2,384,256]{2,1,0:T(8,128)(2,1)}, bf16[2,384,256]{2,1,0:T(8,128)(2,1)}) custom-call(bf16[1536,768]{1,0:T(8,128)(2,1)} %shard_map.87.h1, bf16[1536,640]{1,0:T(8,128)(2,1)} %shard_map.88.h2, bf16[704,256]{1,0:T(8,128)(2,1)} %copy-done.42, ...), custom_call_target="tpu_custom_call" | custom-call | flops 2214592512 | bytes 5898240 | tf_op jit(solution)/shard_map/pallas_call | solution.py:60
  179.7 3.0 %collective-permute-done.48.ax_got.refs_1_ = bf16[2,384,512]{2,1,0:T(8,128)(2,1)S(1)} collective-permute-done((bf16[2,384,512]{2,1,0:T(8,128)(2,1)}, bf16[2,384,512]{2,1,0:T(8,128)(2,1)S(1)}, u32[]{:S(2)}, u32[]{:S(2)}) %collective-permute-start.48) | collective-permute-done | bytes 786464 | tf_op jit(solution)/shard_map/ppermute | solution.py:284
  182.7 1.2 collective-permute-done.51.ay_got.refs_4_
  183.9 1.0 copy-done.1
  184.8 2.4 %shard_map.91 = (bf16[384,512]{1,0:T(8,128)(2,1)}, bf16[384,512]{1,0:T(8,128)(2,1)}) custom-call(bf16[2,384,512]{2,1,0:T(8,128)(2,1)} %get-tuple-element.140.ax_keep.refs_0_, bf16[2,384,512]{2,1,0:T(8,128)(2,1)} %copy-done, bf16[2,384,512]{2,1,0:T(8,128)(2,1)} %get-tuple-element.119.ay_keep.refs_3_, bf16[2,384,512]{2,1,0:T(8,128)(2,1)} %copy-done.1), custom_call_target="tpu_custom_call" | custom-call | flops 786432 | bytes 2359296 | tf_op jit(solution)/shard_map/pallas_call | solution.py:60
  187.2 1.5 collective-permute-done.46.refs_2_
  189.2 1.5 collective-permute-start.55
  192.7 7.0 %shard_map.92 = (bf16[2,384,256]{2,1,0:T(8,128)(2,1)}, bf16[2,384,256]{2,1,0:T(8,128)(2,1)}, bf16[2,384,256]{2,1,0:T(8,128)(2,1)}, bf16[2,384,256]{2,1,0:T(8,128)(2,1)}) custom-call(bf16[1536,768]{1,0:T(8,128)(2,1)} %shard_map.87.h1, bf16[1536,640]{1,0:T(8,128)(2,1)} %shard_map.88.h2, bf16[704,256]{1,0:T(8,128)(2,1)} %copy-done.45, ...), custom_call_target="tpu_custom_call" | custom-call | flops 2214592512 | bytes 5898240 | tf_op jit(solution)/shard_map/pallas_call | solution.py:60
  199.7 0.9 collective-permute-start.54
  200.6 1.2 collective-permute-start.57
  201.8 0.8 collective-permute-start.60
  202.6 1.2 collective-permute-start.61
  203.9 0.7 copy-done.3
  204.6 2.0 shard_map.93
  206.7 1.5 collective-permute-start.62
  208.2 3.8 %collective-permute-done.54.ax_got.refs_1_ = bf16[2,384,256]{2,1,0:T(8,128)(2,1)S(1)} collective-permute-done((bf16[2,384,256]{2,1,0:T(8,128)(2,1)}, bf16[2,384,256]{2,1,0:T(8,128)(2,1)S(1)}, u32[]{:S(2)}, u32[]{:S(2)}) %collective-permute-start.54) | collective-permute-done | bytes 393248 | tf_op jit(solution)/shard_map/ppermute | solution.py:284
  212.0 0.9 collective-permute-start.63
  213.6 2.0 shard_map.94
  215.6 1.2 collective-permute-start.58
  216.8 4.4 %collective-permute-done.60.refs_2_ = bf16[384,512]{1,0:T(8,128)(2,1)S(1)} collective-permute-done((bf16[384,512]{1,0:T(8,128)(2,1)S(1)}, bf16[384,512]{1,0:T(8,128)(2,1)S(1)}, u32[]{:S(2)}, u32[]{:S(2)}) %collective-permute-start.60) | collective-permute-done | bytes 393248 | tf_op jit(solution)/shard_map/ppermute | solution.py:284
  221.2 1.2 collective-permute-start.59
  222.4 3.0 %collective-permute-done.62.refs_8_ = bf16[384,256]{1,0:T(8,128)(2,1)S(1)} collective-permute-done((bf16[384,256]{1,0:T(8,128)(2,1)}, bf16[384,256]{1,0:T(8,128)(2,1)S(1)}, u32[]{:S(2)}, u32[]{:S(2)}) %collective-permute-start.62) | collective-permute-done | bytes 196640 | tf_op jit(solution)/shard_map/ppermute | solution.py:284
  226.2 3.2 %shard_map.95.refs_7_ = bf16[384,2048]{1,0:T(8,128)(2,1)} custom-call(bf16[2,384,512]{2,1,0:T(8,128)(2,1)} %get-tuple-element.140.ax_keep.refs_0_, bf16[2,384,512]{2,1,0:T(8,128)(2,1)} %copy-done, bf16[384,512]{1,0:T(8,128)(2,1)} %copy-done.6, bf16[2,384,512]{2,1,0:T(8,128)(2,1)} %get-tuple-element.119.ay_keep.refs_3_, bf16[2,384,512]{2,1,0:T(8,128)(2,1)} %copy-done.1, ...), custom_call_target="tpu_custom_call" | custom-call | flops 2359296 | bytes 4718592 | tf_op jit(solution)/shard_map/pallas_call | solution.py:60
  230.8 2.2 shard_map.96
  (194 shorter events, 16.8 us)
Async XLA Ops:
  2.0 13.9 %collective-permute-start.2 = (bf16[256,768]{1,0:T(8,128)(2,1)}, bf16[256,768]{1,0:T(8,128)(2,1)S(1)}, u32[]{:S(2)}, u32[]{:S(2)}) collective-permute-start(bf16[256,768]{1,0:T(8,128)(2,1)} %shard_map.82.refs_8_), channel_id=1, source_target_pairs={{0,8},{8,12},{12,4},{4,0},{1,9},{9,13},{13,5},{5,1},{2,10},{10,14}... | collective-permute-start | bytes 1179656 | tf_op jit(solution)/shard_map/ppermute | solution.py:284
  8.8 13.5 %collective-permute-start.1 = (bf16[256,768]{1,0:T(8,128)(2,1)}, bf16[256,768]{1,0:T(8,128)(2,1)}, u32[]{:S(2)}, u32[]{:S(2)}) collective-permute-start(bf16[256,768]{1,0:T(8,128)(2,1)} %get-tuple-element.83), channel_id=1, source_target_pairs={{0,2},{2,0},{1,3},{3,1},{4,6},{6,4},{5,7},{7,5},{8,10},{10,8},{9,1... | collective-permute-start | bytes 1179656 | tf_op jit(solution)/shard_map/ppermute | solution.py:284
  10.3 12.0 %collective-permute-start.6 = (bf16[256,640]{1,0:T(8,128)(2,1)}, bf16[256,640]{1,0:T(8,128)(2,1)}, u32[]{:S(2)}, u32[]{:S(2)}) collective-permute-start(bf16[256,640]{1,0:T(8,128)(2,1)} %get-tuple-element.75.refs_8_), channel_id=1, source_target_pairs={{0,8},{8,12},{12,4},{4,0},{1,9},{9,13},{13,5},{5,1},{2,10},{10,14}... | collective-permute-start | bytes 983048 | tf_op jit(solution)/shard_map/ppermute | solution.py:284
  11.9 16.2 %collective-permute-start.5 = (bf16[256,640]{1,0:T(8,128)(2,1)}, bf16[256,640]{1,0:T(8,128)(2,1)S(1)}, u32[]{:S(2)}, u32[]{:S(2)}) collective-permute-start(bf16[256,640]{1,0:T(8,128)(2,1)} %get-tuple-element.86), channel_id=1, source_target_pairs={{0,2},{2,0},{1,3},{3,1},{4,6},{6,4},{5,7},{7,5},{8,10},{10,8},{9,1... | collective-permute-start | bytes 983048 | tf_op jit(solution)/shard_map/ppermute | solution.py:284
  12.5 19.9 %collective-permute-start.20 = (bf16[256,768]{1,0:T(8,128)(2,1)S(1)}, bf16[256,768]{1,0:T(8,128)(2,1)}, u32[]{:S(2)}, u32[]{:S(2)}) collective-permute-start(bf16[256,768]{1,0:T(8,128)(2,1)S(1)} %copy-done.8), channel_id=1, source_target_pairs={{0,1},{1,0},{2,3},{3,2},{4,5},{5,4},{6,7},{7,6},{8,9},{9,8},{10,11... | collective-permute-start | bytes 1179656 | tf_op jit(solution)/shard_map/ppermute | solution.py:284
  16.6 41.2 %collective-permute-start.9 = (bf16[256,2048]{1,0:T(8,128)(2,1)}, bf16[256,2048]{1,0:T(8,128)(2,1)S(1)}, u32[]{:S(2)}, u32[]{:S(2)}) collective-permute-start(bf16[256,2048]{1,0:T(8,128)(2,1)} %get-tuple-element.77.refs_1_), channel_id=1, source_target_pairs={{0,2},{2,0},{1,3},{3,1},{4,6},{6,4},{5,7},{7,5},{8,10},{10,8},{9,1... | collective-permute-start | bytes 3145736 | tf_op jit(solution)/shard_map/ppermute | solution.py:284
  28.1 16.1 %collective-permute-start.11 = (bf16[256,640]{1,0:T(8,128)(2,1)S(1)}, bf16[256,640]{1,0:T(8,128)(2,1)S(1)}, u32[]{:S(2)}, u32[]{:S(2)}) collective-permute-start(bf16[256,640]{1,0:T(8,128)(2,1)S(1)} %collective-permute-done.5.refs_12_), channel_id=1, source_target_pairs={{8,0},{12,8},{4,12},{0,4},{9,1},{13,9},{5,13},{1,5},{10,2},{14,10}... | collective-permute-start | bytes 983048 | tf_op jit(solution)/shard_map/ppermute | solution.py:284
  28.1 18.4 %collective-permute-start.4 = (bf16[256,768]{1,0:T(8,128)(2,1)}, bf16[256,768]{1,0:T(8,128)(2,1)S(1)}, u32[]{:S(2)}, u32[]{:S(2)}) collective-permute-start(bf16[256,768]{1,0:T(8,128)(2,1)} %copy-done.24), channel_id=1, source_target_pairs={{0,8},{8,12},{12,4},{4,0},{1,9},{9,13},{13,5},{5,1},{2,10},{10,14}... | collective-permute-start | bytes 1179656 | tf_op jit(solution)/shard_map/ppermute | solution.py:284
  31.0 1.4 collective-permute-start
  32.4 20.5 %collective-permute-start.3 = (bf16[256,768]{1,0:T(8,128)(2,1)}, bf16[256,768]{1,0:T(8,128)(2,1)S(1)}, u32[]{:S(2)}, u32[]{:S(2)}) collective-permute-start(bf16[256,768]{1,0:T(8,128)(2,1)} %collective-permute-done.1.refs_12_), channel_id=1, source_target_pairs={{8,0},{12,8},{4,12},{0,4},{9,1},{13,9},{5,13},{1,5},{10,2},{14,10}... | collective-permute-start | bytes 1179656 | tf_op jit(solution)/shard_map/ppermute | solution.py:284
  32.4 24.0 %collective-permute-start.10 = (bf16[128,2048]{1,0:T(8,128)(2,1)S(1)}, bf16[128,2048]{1,0:T(8,128)(2,1)S(1)}, u32[]{:S(2)}, u32[]{:S(2)}) collective-permute-start(bf16[128,2048]{1,0:T(8,128)(2,1)S(1)} %copy-done.20), channel_id=1, source_target_pairs={{0,16},{16,0},{1,17},{17,1},{2,18},{18,2},{3,19},{19,3},{4,20},{20... | collective-permute-start | bytes 1572872 | tf_op jit(solution)/shard_map/ppermute | solution.py:284
  44.2 10.2 %collective-permute-start.24 = (bf16[256,768]{1,0:T(8,128)(2,1)}, bf16[256,768]{1,0:T(8,128)(2,1)S(1)}, u32[]{:S(2)}, u32[]{:S(2)}) collective-permute-start(bf16[256,768]{1,0:T(8,128)(2,1)} %collective-permute-done.1.refs_12_), channel_id=1, source_target_pairs={{0,1},{1,0},{2,3},{3,2},{4,5},{5,4},{6,7},{7,6},{8,9},{9,8},{10,11... | collective-permute-start | bytes 1179656 | tf_op jit(solution)/shard_map/ppermute | solution.py:284
  46.5 8.4 %collective-permute-start.21 = (bf16[256,768]{1,0:T(8,128)(2,1)}, bf16[256,768]{1,0:T(8,128)(2,1)}, u32[]{:S(2)}, u32[]{:S(2)}) collective-permute-start(bf16[256,768]{1,0:T(8,128)(2,1)} %copy-done.24), channel_id=1, source_target_pairs={{0,1},{1,0},{2,3},{3,2},{4,5},{5,4},{6,7},{7,6},{8,9},{9,8},{10,11... | collective-permute-start | bytes 1179656 | tf_op jit(solution)/shard_map/ppermute | solution.py:284
  52.8 12.2 %collective-permute-start.16 = (bf16[128,2048]{1,0:T(8,128)(2,1)S(1)}, bf16[128,2048]{1,0:T(8,128)(2,1)S(1)}, u32[]{:S(2)}, u32[]{:S(2)}) collective-permute-start(bf16[128,2048]{1,0:T(8,128)(2,1)S(1)} %copy-done.20), channel_id=1, source_target_pairs={{0,2},{2,0},{1,3},{3,1},{4,6},{6,4},{5,7},{7,5},{8,10},{10,8},{9,1... | collective-permute-start | bytes 1572872 | tf_op jit(solution)/shard_map/ppermute | solution.py:284
  54.3 20.5 %collective-permute-start.8 = (bf16[256,768]{1,0:T(8,128)(2,1)S(1)}, bf16[256,768]{1,0:T(8,128)(2,1)S(1)}, u32[]{:S(2)}, u32[]{:S(2)}) collective-permute-start(bf16[256,768]{1,0:T(8,128)(2,1)S(1)} %collective-permute-done.4.refs_10_), channel_id=1, source_target_pairs={{0,8},{8,12},{12,4},{4,0},{1,9},{9,13},{13,5},{5,1},{2,10},{10,14}... | collective-permute-start | bytes 1179656 | tf_op jit(solution)/shard_map/ppermute | solution.py:284
  54.9 44.6 %collective-permute-start.17 = (bf16[256,2048]{1,0:T(8,128)(2,1)S(1)}, bf16[256,2048]{1,0:T(8,128)(2,1)S(1)}, u32[]{:S(2)}, u32[]{:S(2)}) collective-permute-start(bf16[256,2048]{1,0:T(8,128)(2,1)S(1)} %copy-done.16), channel_id=1, source_target_pairs={{0,16},{16,0},{1,17},{17,1},{2,18},{18,2},{3,19},{19,3},{4,20},{20... | collective-permute-start | bytes 3145736 | tf_op jit(solution)/shard_map/ppermute | solution.py:284
  56.4 19.9 %collective-permute-start.7 = (bf16[256,768]{1,0:T(8,128)(2,1)S(1)}, bf16[256,768]{1,0:T(8,128)(2,1)S(1)}, u32[]{:S(2)}, u32[]{:S(2)}) collective-permute-start(bf16[256,768]{1,0:T(8,128)(2,1)S(1)} %collective-permute-done.3.refs_13_), channel_id=1, source_target_pairs={{8,0},{12,8},{4,12},{0,4},{9,1},{13,9},{5,13},{1,5},{10,2},{14,10}... | collective-permute-start | bytes 1179656 | tf_op jit(solution)/shard_map/ppermute | solution.py:284
  57.9 32.4 %collective-permute-start.15 = (bf16[256,640]{1,0:T(8,128)(2,1)}, bf16[256,640]{1,0:T(8,128)(2,1)}, u32[]{:S(2)}, u32[]{:S(2)}) collective-permute-start(bf16[256,640]{1,0:T(8,128)(2,1)} %collective-permute-done.6.refs_9_), channel_id=1, source_target_pairs={{0,8},{8,12},{12,4},{4,0},{1,9},{9,13},{13,5},{5,1},{2,10},{10,14}... | collective-permute-start | bytes 983048 | tf_op jit(solution)/shard_map/ppermute | solution.py:284
  65.1 25.3 %collective-permute-start.13 = (bf16[704,256]{1,0:T(8,128)(2,1)}, bf16[704,256]{1,0:T(8,128)(2,1)S(1)}, u32[]{:S(2)}, u32[]{:S(2)}) collective-permute-start(bf16[704,256]{1,0:T(8,128)(2,1)} %get-tuple-element.98), channel_id=1, source_target_pairs={{0,2},{2,0},{1,3},{3,1},{4,6},{6,4},{5,7},{7,5},{8,10},{10,8},{9,1... | collective-permute-start | bytes 1081352 | tf_op jit(solution)/shard_map/ppermute | solution.py:284
  74.8 15.5 %collective-permute-start.14 = (bf16[256,640]{1,0:T(8,128)(2,1)S(1)}, bf16[256,640]{1,0:T(8,128)(2,1)}, u32[]{:S(2)}, u32[]{:S(2)}) collective-permute-start(bf16[256,640]{1,0:T(8,128)(2,1)S(1)} %collective-permute-done.11.refs_13_), channel_id=1, source_target_pairs={{8,0},{12,8},{4,12},{0,4},{9,1},{13,9},{5,13},{1,5},{10,2},{14,10}... | collective-permute-start | bytes 983048 | tf_op jit(solution)/shard_map/ppermute | solution.py:284
  76.4 32.4 %collective-permute-start.19 = (bf16[256,2048]{1,0:T(8,128)(2,1)S(1)}, bf16[256,2048]{1,0:T(8,128)(2,1)S(1)}, u32[]{:S(2)}, u32[]{:S(2)}) collective-permute-start(bf16[256,2048]{1,0:T(8,128)(2,1)S(1)} %collective-permute-done.9.refs_3_), channel_id=1, source_target_pairs={{0,16},{16,0},{1,17},{17,1},{2,18},{18,2},{3,19},{19,3},{4,20},{20... | collective-permute-start | bytes 3145736 | tf_op jit(solution)/shard_map/ppermute | solution.py:284
  90.3 8.7 %collective-permute-start.12 = (bf16[256,768]{1,0:T(8,128)(2,1)S(1)}, bf16[256,768]{1,0:T(8,128)(2,1)S(1)}, u32[]{:S(2)}, u32[]{:S(2)}) collective-permute-start(bf16[256,768]{1,0:T(8,128)(2,1)S(1)} %collective-permute-done.7.refs_14_), channel_id=1, source_target_pairs={{8,0},{12,8},{4,12},{0,4},{9,1},{13,9},{5,13},{1,5},{10,2},{14,10}... | collective-permute-start | bytes 1179656 | tf_op jit(solution)/shard_map/ppermute | solution.py:284
  90.3 9.2 %collective-permute-start.25 = (bf16[256,768]{1,0:T(8,128)(2,1)S(1)}, bf16[256,768]{1,0:T(8,128)(2,1)S(1)}, u32[]{:S(2)}, u32[]{:S(2)}) collective-permute-start(bf16[256,768]{1,0:T(8,128)(2,1)S(1)} %collective-permute-done.3.refs_13_), channel_id=1, source_target_pairs={{0,1},{1,0},{2,3},{3,2},{4,5},{5,4},{6,7},{7,6},{8,9},{9,8},{10,11... | collective-permute-start | bytes 1179656 | tf_op jit(solution)/shard_map/ppermute | solution.py:284
  90.4 9.6 %collective-permute-start.22 = (bf16[256,768]{1,0:T(8,128)(2,1)S(1)}, bf16[256,768]{1,0:T(8,128)(2,1)S(1)}, u32[]{:S(2)}, u32[]{:S(2)}) collective-permute-start(bf16[256,768]{1,0:T(8,128)(2,1)S(1)} %collective-permute-done.4.refs_10_), channel_id=1, source_target_pairs={{0,1},{1,0},{2,3},{3,2},{4,5},{5,4},{6,7},{7,6},{8,9},{9,8},{10,11... | collective-permute-start | bytes 1179656 | tf_op jit(solution)/shard_map/ppermute | solution.py:284
  99.0 9.2 %collective-permute-start.18 = (bf16[128,2048]{1,0:T(8,128)(2,1)S(1)}, bf16[128,2048]{1,0:T(8,128)(2,1)S(1)}, u32[]{:S(2)}, u32[]{:S(2)}) collective-permute-start(bf16[128,2048]{1,0:T(8,128)(2,1)S(1)} %collective-permute-done.10.refs_4_), channel_id=1, source_target_pairs={{0,2},{2,0},{1,3},{3,1},{4,6},{6,4},{5,7},{7,5},{8,10},{10,8},{9,1... | collective-permute-start | bytes 1572872 | tf_op jit(solution)/shard_map/ppermute | solution.py:284
  99.5 8.6 %collective-permute-start.26 = (bf16[256,768]{1,0:T(8,128)(2,1)S(1)}, bf16[256,768]{1,0:T(8,128)(2,1)S(1)}, u32[]{:S(2)}, u32[]{:S(2)}) collective-permute-start(bf16[256,768]{1,0:T(8,128)(2,1)S(1)} %collective-permute-done.7.refs_14_), channel_id=1, source_target_pairs={{0,1},{1,0},{2,3},{3,2},{4,5},{5,4},{6,7},{7,6},{8,9},{9,8},{10,11... | collective-permute-start | bytes 1179656 | tf_op jit(solution)/shard_map/ppermute | solution.py:284
  99.5 9.1 %collective-permute-start.23 = (bf16[256,768]{1,0:T(8,128)(2,1)S(1)}, bf16[256,768]{1,0:T(8,128)(2,1)S(1)}, u32[]{:S(2)}, u32[]{:S(2)}) collective-permute-start(bf16[256,768]{1,0:T(8,128)(2,1)S(1)} %collective-permute-done.8.refs_11_), channel_id=1, source_target_pairs={{0,1},{1,0},{2,3},{3,2},{4,5},{5,4},{6,7},{7,6},{8,9},{9,8},{10,11... | collective-permute-start | bytes 1179656 | tf_op jit(solution)/shard_map/ppermute | solution.py:284
  100.0 8.7 %collective-permute-start.27 = (bf16[256,768]{1,0:T(8,128)(2,1)S(1)}, bf16[256,768]{1,0:T(8,128)(2,1)S(1)}, u32[]{:S(2)}, u32[]{:S(2)}) collective-permute-start(bf16[256,768]{1,0:T(8,128)(2,1)S(1)} %collective-permute-done.12.refs_15_), channel_id=1, source_target_pairs={{0,1},{1,0},{2,3},{3,2},{4,5},{5,4},{6,7},{7,6},{8,9},{9,8},{10,11... | collective-permute-start | bytes 1179656 | tf_op jit(solution)/shard_map/ppermute | solution.py:284
  108.1 21.1 %collective-permute-start.32 = (bf16[256,640]{1,0:T(8,128)(2,1)}, bf16[256,640]{1,0:T(8,128)(2,1)}, u32[]{:S(2)}, u32[]{:S(2)}) collective-permute-start(bf16[256,640]{1,0:T(8,128)(2,1)} %get-tuple-element.75.refs_8_), channel_id=1, source_target_pairs={{0,1},{1,0},{2,3},{3,2},{4,5},{5,4},{6,7},{7,6},{8,9},{9,8},{10,11... | collective-permute-start | bytes 983048 | tf_op jit(solution)/shard_map/ppermute | solution.py:284
  108.2 21.1 %collective-permute-start.36 = (bf16[256,640]{1,0:T(8,128)(2,1)}, bf16[256,640]{1,0:T(8,128)(2,1)}, u32[]{:S(2)}, u32[]{:S(2)}) collective-permute-start(bf16[256,640]{1,0:T(8,128)(2,1)} %copy-done.51), channel_id=1, source_target_pairs={{0,1},{1,0},{2,3},{3,2},{4,5},{5,4},{6,7},{7,6},{8,9},{9,8},{10,11... | collective-permute-start | bytes 983048 | tf_op jit(solution)/shard_map/ppermute | solution.py:284
  108.7 21.1 %collective-permute-start.33 = (bf16[256,640]{1,0:T(8,128)(2,1)}, bf16[256,640]{1,0:T(8,128)(2,1)}, u32[]{:S(2)}, u32[]{:S(2)}) collective-permute-start(bf16[256,640]{1,0:T(8,128)(2,1)} %collective-permute-done.6.refs_9_), channel_id=1, source_target_pairs={{0,1},{1,0},{2,3},{3,2},{4,5},{5,4},{6,7},{7,6},{8,9},{9,8},{10,11... | collective-permute-start | bytes 983048 | tf_op jit(solution)/shard_map/ppermute | solution.py:284
  108.8 19.9 %collective-permute-start.31 = (bf16[256,640]{1,0:T(8,128)(2,1)}, bf16[256,640]{1,0:T(8,128)(2,1)}, u32[]{:S(2)}, u32[]{:S(2)}) collective-permute-start(bf16[256,640]{1,0:T(8,128)(2,1)} %collective-permute-done.15.refs_10_), channel_id=1, source_target_pairs={{0,8},{8,12},{12,4},{4,0},{1,9},{9,13},{13,5},{5,1},{2,10},{10,14}... | collective-permute-start | bytes 983048 | tf_op jit(solution)/shard_map/ppermute | solution.py:284
  110.6 18.1 %collective-permute-start.30 = (bf16[256,640]{1,0:T(8,128)(2,1)}, bf16[256,640]{1,0:T(8,128)(2,1)}, u32[]{:S(2)}, u32[]{:S(2)}) collective-permute-start(bf16[256,640]{1,0:T(8,128)(2,1)} %collective-permute-done.14.refs_14_), channel_id=1, source_target_pairs={{8,0},{12,8},{4,12},{0,4},{9,1},{13,9},{5,13},{1,5},{10,2},{14,10}... | collective-permute-start | bytes 983048 | tf_op jit(solution)/shard_map/ppermute | solution.py:284
  128.6 1.9 collective-permute-start.37
  128.7 3.4 %collective-permute-start.38 = (bf16[256,640]{1,0:T(8,128)(2,1)}, bf16[256,640]{1,0:T(8,128)(2,1)S(1)}, u32[]{:S(2)}, u32[]{:S(2)}) collective-permute-start(bf16[256,640]{1,0:T(8,128)(2,1)} %collective-permute-done.14.refs_14_), channel_id=1, source_target_pairs={{0,1},{1,0},{2,3},{3,2},{4,5},{5,4},{6,7},{7,6},{8,9},{9,8},{10,11... | collective-permute-start | bytes 983048 | tf_op jit(solution)/shard_map/ppermute | solution.py:284
  129.2 3.0 %collective-permute-start.34 = (bf16[256,640]{1,0:T(8,128)(2,1)}, bf16[256,640]{1,0:T(8,128)(2,1)S(1)}, u32[]{:S(2)}, u32[]{:S(2)}) collective-permute-start(bf16[256,640]{1,0:T(8,128)(2,1)} %collective-permute-done.15.refs_10_), channel_id=1, source_target_pairs={{0,1},{1,0},{2,3},{3,2},{4,5},{5,4},{6,7},{7,6},{8,9},{9,8},{10,11... | collective-permute-start | bytes 983048 | tf_op jit(solution)/shard_map/ppermute | solution.py:284
  129.3 3.3 %collective-permute-start.39 = (bf16[256,640]{1,0:T(8,128)(2,1)}, bf16[256,640]{1,0:T(8,128)(2,1)}, u32[]{:S(2)}, u32[]{:S(2)}) collective-permute-start(bf16[256,640]{1,0:T(8,128)(2,1)} %collective-permute-done.30.refs_15_), channel_id=1, source_target_pairs={{0,1},{1,0},{2,3},{3,2},{4,5},{5,4},{6,7},{7,6},{8,9},{9,8},{10,11... | collective-permute-start | bytes 983048 | tf_op jit(solution)/shard_map/ppermute | solution.py:284
  129.7 3.1 %collective-permute-start.35 = (bf16[256,640]{1,0:T(8,128)(2,1)}, bf16[256,640]{1,0:T(8,128)(2,1)}, u32[]{:S(2)}, u32[]{:S(2)}) collective-permute-start(bf16[256,640]{1,0:T(8,128)(2,1)} %collective-permute-done.31.refs_11_), channel_id=1, source_target_pairs={{0,1},{1,0},{2,3},{3,2},{4,5},{5,4},{6,7},{7,6},{8,9},{9,8},{10,11... | collective-permute-start | bytes 983048 | tf_op jit(solution)/shard_map/ppermute | solution.py:284
  130.5 17.7 %collective-permute-start.29 = (bf16[704,256]{1,0:T(8,128)(2,1)S(1)}, bf16[704,256]{1,0:T(8,128)(2,1)S(1)}, u32[]{:S(2)}, u32[]{:S(2)}) collective-permute-start(bf16[704,256]{1,0:T(8,128)(2,1)S(1)} %get-tuple-element.143.refs_0_), channel_id=1, source_target_pairs={{0,8},{8,12},{12,4},{4,0},{1,9},{9,13},{13,5},{5,1},{2,10},{10,14}... | collective-permute-start | bytes 1081352 | tf_op jit(solution)/shard_map/ppermute | solution.py:284
  132.2 19.1 %collective-permute-start.42 = (bf16[704,256]{1,0:T(8,128)(2,1)S(1)}, bf16[704,256]{1,0:T(8,128)(2,1)S(1)}, u32[]{:S(2)}, u32[]{:S(2)}) collective-permute-start(bf16[704,256]{1,0:T(8,128)(2,1)S(1)} %get-tuple-element.143.refs_0_), channel_id=1, source_target_pairs={{0,1},{1,0},{2,3},{3,2},{4,5},{5,4},{6,7},{7,6},{8,9},{9,8},{10,11... | collective-permute-start | bytes 1081352 | tf_op jit(solution)/shard_map/ppermute | solution.py:284
  132.2 16.9 %collective-permute-start.28 = (bf16[704,256]{1,0:T(8,128)(2,1)S(1)}, bf16[704,256]{1,0:T(8,128)(2,1)S(1)}, u32[]{:S(2)}, u32[]{:S(2)}) collective-permute-start(bf16[704,256]{1,0:T(8,128)(2,1)S(1)} %get-tuple-element.144.refs_2_), channel_id=1, source_target_pairs={{8,0},{12,8},{4,12},{0,4},{9,1},{13,9},{5,13},{1,5},{10,2},{14,10}... | collective-permute-start | bytes 1081352 | tf_op jit(solution)/shard_map/ppermute | solution.py:284
  132.6 19.0 %collective-permute-start.43 = (bf16[704,256]{1,0:T(8,128)(2,1)S(1)}, bf16[704,256]{1,0:T(8,128)(2,1)S(1)}, u32[]{:S(2)}, u32[]{:S(2)}) collective-permute-start(bf16[704,256]{1,0:T(8,128)(2,1)S(1)} %get-tuple-element.144.refs_2_), channel_id=1, source_target_pairs={{0,1},{1,0},{2,3},{3,2},{4,5},{5,4},{6,7},{7,6},{8,9},{9,8},{10,11... | collective-permute-start | bytes 1081352 | tf_op jit(solution)/shard_map/ppermute | solution.py:284
  149.1 2.6 %collective-permute-start.45 = (bf16[704,256]{1,0:T(8,128)(2,1)S(1)}, bf16[704,256]{1,0:T(8,128)(2,1)S(1)}, u32[]{:S(2)}, u32[]{:S(2)}) collective-permute-start(bf16[704,256]{1,0:T(8,128)(2,1)S(1)} %collective-permute-done.28.refs_6_), channel_id=1, source_target_pairs={{0,1},{1,0},{2,3},{3,2},{4,5},{5,4},{6,7},{7,6},{8,9},{9,8},{10,11... | collective-permute-start | bytes 1081352 | tf_op jit(solution)/shard_map/ppermute | solution.py:284
  149.1 2.5 %collective-permute-start.44 = (bf16[704,256]{1,0:T(8,128)(2,1)S(1)}, bf16[704,256]{1,0:T(8,128)(2,1)}, u32[]{:S(2)}, u32[]{:S(2)}) collective-permute-start(bf16[704,256]{1,0:T(8,128)(2,1)S(1)} %collective-permute-done.29.refs_4_), channel_id=1, source_target_pairs={{0,1},{1,0},{2,3},{3,2},{4,5},{5,4},{6,7},{7,6},{8,9},{9,8},{10,11... | collective-permute-start | bytes 1081352 | tf_op jit(solution)/shard_map/ppermute | solution.py:284
  149.6 15.6 %collective-permute-start.41 = (bf16[704,256]{1,0:T(8,128)(2,1)S(1)}, bf16[704,256]{1,0:T(8,128)(2,1)S(1)}, u32[]{:S(2)}, u32[]{:S(2)}) collective-permute-start(bf16[704,256]{1,0:T(8,128)(2,1)S(1)} %collective-permute-done.29.refs_4_), channel_id=1, source_target_pairs={{0,8},{8,12},{12,4},{4,0},{1,9},{9,13},{13,5},{5,1},{2,10},{10,14}... | collective-permute-start | bytes 1081352 | tf_op jit(solution)/shard_map/ppermute | solution.py:284
  151.2 18.0 %collective-permute-start.40 = (bf16[704,256]{1,0:T(8,128)(2,1)S(1)}, bf16[704,256]{1,0:T(8,128)(2,1)S(1)}, u32[]{:S(2)}, u32[]{:S(2)}) collective-permute-start(bf16[704,256]{1,0:T(8,128)(2,1)S(1)} %collective-permute-done.28.refs_6_), channel_id=1, source_target_pairs={{8,0},{12,8},{4,12},{0,4},{9,1},{13,9},{5,13},{1,5},{10,2},{14,10}... | collective-permute-start | bytes 1081352 | tf_op jit(solution)/shard_map/ppermute | solution.py:284
  163.1 19.6 %collective-permute-start.48 = (bf16[2,384,512]{2,1,0:T(8,128)(2,1)}, bf16[2,384,512]{2,1,0:T(8,128)(2,1)S(1)}, u32[]{:S(2)}, u32[]{:S(2)}) collective-permute-start(bf16[2,384,512]{2,1,0:T(8,128)(2,1)} %get-tuple-element.115), channel_id=1, source_target_pairs={{0,16},{16,0},{1,17},{17,1},{2,18},{18,2},{3,19},{19,3},{4,20},{20... | collective-permute-start | bytes 2359304 | tf_op jit(solution)/shard_map/ppermute | solution.py:284
  164.6 19.2 %collective-permute-start.51 = (bf16[2,384,512]{2,1,0:T(8,128)(2,1)}, bf16[2,384,512]{2,1,0:T(8,128)(2,1)S(1)}, u32[]{:S(2)}, u32[]{:S(2)}) collective-permute-start(bf16[2,384,512]{2,1,0:T(8,128)(2,1)} %get-tuple-element.120), channel_id=1, source_target_pairs={{0,2},{2,0},{1,3},{3,1},{4,6},{6,4},{5,7},{7,5},{8,10},{10,8},{9,1... | collective-permute-start | bytes 2359304 | tf_op jit(solution)/shard_map/ppermute | solution.py:284
  169.3 1.7 collective-permute-start.50
  169.3 2.5 %collective-permute-start.49 = (bf16[704,256]{1,0:T(8,128)(2,1)S(1)}, bf16[704,256]{1,0:T(8,128)(2,1)S(1)}, u32[]{:S(2)}, u32[]{:S(2)}) collective-permute-start(bf16[704,256]{1,0:T(8,128)(2,1)S(1)} %collective-permute-done.41.refs_0_), channel_id=1, source_target_pairs={{0,1},{1,0},{2,3},{3,2},{4,5},{5,4},{6,7},{7,6},{8,9},{9,8},{10,11... | collective-permute-start | bytes 1081352 | tf_op jit(solution)/shard_map/ppermute | solution.py:284
  169.8 17.4 %collective-permute-start.47 = (bf16[704,256]{1,0:T(8,128)(2,1)S(1)}, bf16[704,256]{1,0:T(8,128)(2,1)S(1)}, u32[]{:S(2)}, u32[]{:S(2)}) collective-permute-start(bf16[704,256]{1,0:T(8,128)(2,1)S(1)} %collective-permute-done.41.refs_0_), channel_id=1, source_target_pairs={{0,8},{8,12},{12,4},{4,0},{1,9},{9,13},{13,5},{5,1},{2,10},{10,14}... | collective-permute-start | bytes 1081352 | tf_op jit(solution)/shard_map/ppermute | solution.py:284
  171.0 17.7 %collective-permute-start.46 = (bf16[704,256]{1,0:T(8,128)(2,1)S(1)}, bf16[704,256]{1,0:T(8,128)(2,1)}, u32[]{:S(2)}, u32[]{:S(2)}) collective-permute-start(bf16[704,256]{1,0:T(8,128)(2,1)S(1)} %collective-permute-done.40.refs_2_), channel_id=1, source_target_pairs={{8,0},{12,8},{4,12},{0,4},{9,1},{13,9},{5,13},{1,5},{10,2},{14,10}... | collective-permute-start | bytes 1081352 | tf_op jit(solution)/shard_map/ppermute | solution.py:284
  188.7 2.5 %collective-permute-start.53 = (bf16[704,256]{1,0:T(8,128)(2,1)}, bf16[704,256]{1,0:T(8,128)(2,1)S(1)}, u32[]{:S(2)}, u32[]{:S(2)}) collective-permute-start(bf16[704,256]{1,0:T(8,128)(2,1)} %collective-permute-done.46.refs_2_), channel_id=1, source_target_pairs={{0,1},{1,0},{2,3},{3,2},{4,5},{5,4},{6,7},{7,6},{8,9},{9,8},{10,11... | collective-permute-start | bytes 1081352 | tf_op jit(solution)/shard_map/ppermute | solution.py:284
  188.7 2.5 %collective-permute-start.52 = (bf16[704,256]{1,0:T(8,128)(2,1)S(1)}, bf16[704,256]{1,0:T(8,128)(2,1)S(1)}, u32[]{:S(2)}, u32[]{:S(2)}) collective-permute-start(bf16[704,256]{1,0:T(8,128)(2,1)S(1)} %collective-permute-done.47.refs_0_), channel_id=1, source_target_pairs={{0,1},{1,0},{2,3},{3,2},{4,5},{5,4},{6,7},{7,6},{8,9},{9,8},{10,11... | collective-permute-start | bytes 1081352 | tf_op jit(solution)/shard_map/ppermute | solution.py:284
  189.2 13.5 %collective-permute-start.55 = (bf16[2,384,256]{2,1,0:T(8,128)(2,1)}, bf16[2,384,256]{2,1,0:T(8,128)(2,1)S(1)}, u32[]{:S(2)}, u32[]{:S(2)}) collective-permute-start(bf16[2,384,256]{2,1,0:T(8,128)(2,1)} %get-tuple-element.128), channel_id=1, source_target_pairs={{0,16},{16,0},{1,17},{17,1},{2,18},{18,2},{3,19},{19,3},{4,20},{20... | collective-permute-start | bytes 1179656 | tf_op jit(solution)/shard_map/ppermute | solution.py:284
  190.7 13.2 %collective-permute-start.56 = (bf16[2,384,256]{2,1,0:T(8,128)(2,1)S(1)}, bf16[2,384,256]{2,1,0:T(8,128)(2,1)S(1)}, u32[]{:S(2)}, u32[]{:S(2)}) collective-permute-start(bf16[2,384,256]{2,1,0:T(8,128)(2,1)S(1)} %copy-done.34), channel_id=1, source_target_pairs={{0,2},{2,0},{1,3},{3,1},{4,6},{6,4},{5,7},{7,5},{8,10},{10,8},{9,1... | collective-permute-start | bytes 1179656 | tf_op jit(solution)/shard_map/ppermute | solution.py:284
  199.7 12.3 %collective-permute-start.54 = (bf16[2,384,256]{2,1,0:T(8,128)(2,1)}, bf16[2,384,256]{2,1,0:T(8,128)(2,1)S(1)}, u32[]{:S(2)}, u32[]{:S(2)}) collective-permute-start(bf16[2,384,256]{2,1,0:T(8,128)(2,1)} %get-tuple-element.127), channel_id=1, source_target_pairs={{0,16},{16,0},{1,17},{17,1},{2,18},{18,2},{3,19},{19,3},{4,20},{20... | collective-permute-start | bytes 1179656 | tf_op jit(solution)/shard_map/ppermute | solution.py:284
  200.6 12.2 %collective-permute-start.57 = (bf16[2,384,256]{2,1,0:T(8,128)(2,1)}, bf16[2,384,256]{2,1,0:T(8,128)(2,1)S(1)}, u32[]{:S(2)}, u32[]{:S(2)}) collective-permute-start(bf16[2,384,256]{2,1,0:T(8,128)(2,1)} %get-tuple-element.136), channel_id=1, source_target_pairs={{0,2},{2,0},{1,3},{3,1},{4,6},{6,4},{5,7},{7,5},{8,10},{10,8},{9,1... | collective-permute-start | bytes 1179656 | tf_op jit(solution)/shard_map/ppermute | solution.py:284
  201.8 19.4 %collective-permute-start.60 = (bf16[384,512]{1,0:T(8,128)(2,1)S(1)}, bf16[384,512]{1,0:T(8,128)(2,1)S(1)}, u32[]{:S(2)}, u32[]{:S(2)}) collective-permute-start(bf16[384,512]{1,0:T(8,128)(2,1)S(1)} %copy-done.31), channel_id=1, source_target_pairs={{0,2},{2,0},{1,3},{3,1},{4,6},{6,4},{5,7},{7,5},{8,10},{10,8},{9,1... | collective-permute-start | bytes 1179656 | tf_op jit(solution)/shard_map/ppermute | solution.py:284
  202.6 19.8 %collective-permute-start.61 = (bf16[384,512]{1,0:T(8,128)(2,1)S(1)}, bf16[384,512]{1,0:T(8,128)(2,1)S(1)}, u32[]{:S(2)}, u32[]{:S(2)}) collective-permute-start(bf16[384,512]{1,0:T(8,128)(2,1)S(1)} %copy-done.30), channel_id=1, source_target_pairs={{0,16},{16,0},{1,17},{17,1},{2,18},{18,2},{3,19},{19,3},{4,20},{20... | collective-permute-start | bytes 1179656 | tf_op jit(solution)/shard_map/ppermute | solution.py:284
  206.7 18.8 %collective-permute-start.62 = (bf16[384,256]{1,0:T(8,128)(2,1)}, bf16[384,256]{1,0:T(8,128)(2,1)S(1)}, u32[]{:S(2)}, u32[]{:S(2)}) collective-permute-start(bf16[384,256]{1,0:T(8,128)(2,1)} %get-tuple-element.133), channel_id=1, source_target_pairs={{0,2},{2,0},{1,3},{3,1},{4,6},{6,4},{5,7},{7,5},{8,10},{10,8},{9,1... | collective-permute-start | bytes 589832 | tf_op jit(solution)/shard_map/ppermute | solution.py:284
  212.0 13.5 %collective-permute-start.63 = (bf16[384,256]{1,0:T(8,128)(2,1)}, bf16[384,256]{1,0:T(8,128)(2,1)S(1)}, u32[]{:S(2)}, u32[]{:S(2)}) collective-permute-start(bf16[384,256]{1,0:T(8,128)(2,1)} %get-tuple-element.142), channel_id=1, source_target_pairs={{0,16},{16,0},{1,17},{17,1},{2,18},{18,2},{3,19},{19,3},{4,20},{20... | collective-permute-start | bytes 589832 | tf_op jit(solution)/shard_map/ppermute | solution.py:284
  215.6 13.8 %collective-permute-start.58 = (bf16[384,256]{1,0:T(8,128)(2,1)}, bf16[384,256]{1,0:T(8,128)(2,1)S(1)}, u32[]{:S(2)}, u32[]{:S(2)}) collective-permute-start(bf16[384,256]{1,0:T(8,128)(2,1)} %get-tuple-element.138), channel_id=1, source_target_pairs={{0,2},{2,0},{1,3},{3,1},{4,6},{6,4},{5,7},{7,5},{8,10},{10,8},{9,1... | collective-permute-start | bytes 589832 | tf_op jit(solution)/shard_map/ppermute | solution.py:284
  221.2 8.2 %collective-permute-start.59 = (bf16[384,256]{1,0:T(8,128)(2,1)}, bf16[384,256]{1,0:T(8,128)(2,1)S(1)}, u32[]{:S(2)}, u32[]{:S(2)}) collective-permute-start(bf16[384,256]{1,0:T(8,128)(2,1)} %get-tuple-element.139), channel_id=1, source_target_pairs={{0,16},{16,0},{1,17},{17,1},{2,18},{18,2},{3,19},{19,3},{4,20},{20... | collective-permute-start | bytes 589832 | tf_op jit(solution)/shard_map/ppermute | solution.py:284
  (57 other events, 782.0 us)
